TPU v7x, 32 devices: a whole 2x2x4 slice. The times are simulated.
32 devices in a mesh: sp: 8 (over z, core), tp: 4 (over y, x).
Axes of the slice: x: 2, y: 2, z: 4, core: 2. Of those that a mesh axis runs over, the one named last changes fastest.
Arguments:
- moe_in: bfloat16 [1536, 2048], P('sp'), may hold values from -6 to 6
- cotangent: bfloat16 [1536, 2048], P('sp'), may hold values from -6 to 6
- routing: int32 [1536, 2], P('sp'), may hold values from 0 to 7, as said below
- route_weight: float32 [1536, 2], P('sp'), may hold values from 0.2 to 1
- w_gate: bfloat16 [8, 2048, 2048], P('sp', 'tp'), may hold values from -0.125 to 0.125
- w_up: bfloat16 [8, 2048, 2048], P('sp', 'tp'), may hold values from -0.125 to 0.125
- w_down: bfloat16 [8, 2048, 2048], P('sp', 'tp'), may hold values from -0.125 to 0.125
- gate_b: bfloat16 [1024, 1536], P('tp', 'sp'), may hold values from -6 to 6
- gate_c: bfloat16 [1024, 1536], P('tp', 'sp'), may hold values from -6 to 6
- value_x: bfloat16 [1024, 1536], P('tp', 'sp'), may hold values from -6 to 6
- conv_taps: float32 [3, 1024], P(None, 'tp'), may hold values from -3 to 3
- out_proj: bfloat16 [1024, 2048], P('tp'), may hold values from -0.1875 to 0.1875
Outputs:
- w_gate_grad: bfloat16 [8, 2048, 2048], P('sp', 'tp')
- w_up_grad: bfloat16 [8, 2048, 2048], P('sp', 'tp')
- w_down_grad: bfloat16 [8, 2048, 2048], P('sp', 'tp')
- moe_in_grad: bfloat16 [1536, 2048], P('sp', 'tp')
- proj_grad: float32 [1024, 2048], P('tp', 'sp')
- gate_b_grad: bfloat16 [1024, 1536], P('tp', 'sp')
- gate_c_grad: bfloat16 [1024, 1536], P('tp', 'sp')
- value_x_grad: bfloat16 [1024, 1536], P('tp', 'sp')
Inputs may be any that keep to these rules, and one draw needn't show every extreme that they name: `routing`: in each aligned block of 192 rows every expert is named exactly 48 times. The two entries of a row are different experts of one group; group g holds experts g * 2 to g * 2 + 1.
All inputs are finite; a program needn't handle non-finite values.
Results may differ from a plain program's by a relative error of at most 0.025.
Values may be sent and summed in bfloat16 or wider, within the bound.
A program may use at most 64 MiB of HBM per device.

v0:
```python
import jax
import jax.numpy as jnp
from jax import lax
from jax.sharding import PartitionSpec as P

TAPS = 3


def from_behind(array, axis, by):
    count = lax.axis_size(axis)
    pairs = [(i, i + by) for i in range(count) if 0 <= i + by < count]
    return lax.ppermute(array, axis, pairs)


def on_device(
    moe_in,
    cotangent,
    routing,
    route_weight,
    w_gate,
    w_up,
    w_down,
    gate_b,
    gate_c,
    value_x,
    conv_taps,
    out_proj,
):
    tok_rows = routing.shape[0]
    top_routes = routing.shape[1]
    experts = lax.axis_size("sp")
    lane_count = lax.axis_size("tp")
    model_width = moe_in.shape[1]
    capacity = top_routes * tok_rows // experts
    flat_routes = routing.reshape(-1)
    route_count = flat_routes.shape[0]
    one_hot = (flat_routes[:, None] == jnp.arange(experts, dtype=jnp.int32)[None, :]).astype(
        jnp.int32
    )
    slot_rank = jnp.sum(jnp.cumsum(one_hot, axis=0) * one_hot, axis=1) - 1
    slot_index = flat_routes * capacity + slot_rank
    source = (
        jnp.zeros((route_count,), jnp.int32)
        .at[slot_index]
        .set(jnp.arange(route_count, dtype=jnp.int32))
    )
    owner_token = source // top_routes
    scales = route_weight.reshape(-1)[source][:, None]
    col_width = model_width // lane_count
    col_start = lax.axis_index("tp") * col_width
    rows_part = lax.dynamic_slice_in_dim(moe_in, col_start, col_width, 1)[owner_token]
    cot_slice = lax.dynamic_slice_in_dim(cotangent, col_start, col_width, 1)[owner_token]
    cot_part = (scales * cot_slice.astype(jnp.float32)).astype(jnp.bfloat16)
    moved = (
        lax.all_to_all(rows_part, "sp", split_axis=0, concat_axis=0, tiled=True),
        lax.all_to_all(cot_part, "sp", split_axis=0, concat_axis=0, tiled=True),
    )
    arrived, arrived_cot = (
        lax.all_gather(moved[0], "tp", axis=1, tiled=True),
        lax.all_gather(moved[1], "tp", axis=1, tiled=True),
    )
    contract_model = (((1,), (1,)), ((), ()))
    over_rows = (((0,), (0,)), ((), ()))
    gate_pre = lax.dot_general(
        arrived, w_gate[0], contract_model, preferred_element_type=jnp.float32
    )
    up_pre = lax.dot_general(arrived, w_up[0], contract_model, preferred_element_type=jnp.float32)
    sigmoid_gate = jax.nn.sigmoid(gate_pre)
    hidden = (gate_pre * sigmoid_gate * up_pre).astype(jnp.bfloat16)
    hidden_grad = lax.dot_general(
        arrived_cot, w_down[0], contract_model, preferred_element_type=jnp.float32
    )
    gate_grad = (
        hidden_grad * up_pre * sigmoid_gate * (1.0 + gate_pre * (1.0 - sigmoid_gate))
    ).astype(jnp.bfloat16)
    up_grad = (hidden_grad * gate_pre * sigmoid_gate).astype(jnp.bfloat16)
    w_gate_grad = lax.dot_general(
        gate_grad, arrived, over_rows, preferred_element_type=jnp.float32
    ).astype(jnp.bfloat16)[None]
    w_up_grad = lax.dot_general(
        up_grad, arrived, over_rows, preferred_element_type=jnp.float32
    ).astype(jnp.bfloat16)[None]
    w_down_grad = lax.dot_general(
        hidden, arrived_cot, over_rows, preferred_element_type=jnp.float32
    ).astype(jnp.bfloat16)[None]
    partial_value = jnp.dot(gate_grad, w_gate[0], preferred_element_type=jnp.float32) + jnp.dot(
        up_grad, w_up[0], preferred_element_type=jnp.float32
    )
    partial_value = lax.optimization_barrier(partial_value.astype(jnp.bfloat16)).astype(jnp.float32)
    summed = lax.psum_scatter(
        partial_value.astype(jnp.bfloat16), "tp", scatter_dimension=1, tiled=True
    )
    returned = lax.all_to_all(summed, "sp", split_axis=0, concat_axis=0, tiled=True)
    per_route = returned[slot_index].astype(jnp.float32)
    moe_in_grad = jnp.sum(per_route.reshape(tok_rows, top_routes, -1), axis=1).astype(jnp.bfloat16)
    full_grad = lax.all_gather(moe_in_grad, "tp", axis=1, tiled=True)
    stream_grad = (cotangent.astype(jnp.float32) + full_grad.astype(jnp.float32)).astype(
        jnp.bfloat16
    )
    mixed_in = lax.optimization_barrier(
        (gate_c.astype(jnp.float32) * value_x.astype(jnp.float32)).astype(jnp.bfloat16)
    )
    earlier = from_behind(mixed_in[:, tok_rows - (TAPS - 1) :], "sp", 1)
    extended = jnp.concatenate([earlier, mixed_in], axis=1).astype(jnp.float32)
    conv_out = jnp.zeros(mixed_in.shape, jnp.float32)
    for tap in range(TAPS):
        conv_out = conv_out + conv_taps[tap][:, None] * extended[:, tap : tap + tok_rows]
    mixer_act = (gate_b.astype(jnp.float32) * conv_out).astype(jnp.bfloat16)
    act_grad = lax.dot_general(
        out_proj, stream_grad, contract_model, preferred_element_type=jnp.float32
    )
    proj_rows = lax.psum_scatter(
        lax.dot_general(
            stream_grad, mixer_act, (((0,), (1,)), ((), ())), preferred_element_type=jnp.float32
        ).astype(jnp.bfloat16),
        "sp",
        scatter_dimension=0,
        tiled=True,
    ).astype(jnp.float32)
    proj_grad = proj_rows.T
    gate_b_grad = (act_grad * conv_out).astype(jnp.bfloat16)
    conv_grad = act_grad * gate_b.astype(jnp.float32)
    later = from_behind(conv_grad[:, : TAPS - 1], "sp", -1)
    extended_grad = jnp.concatenate([conv_grad, later], axis=1)
    mixed_grad = jnp.zeros(conv_grad.shape, jnp.float32)
    for tap in range(TAPS):
        offset = TAPS - 1 - tap
        mixed_grad = (
            mixed_grad + conv_taps[tap][:, None] * extended_grad[:, offset : offset + tok_rows]
        )
    gate_c_grad = (mixed_grad * value_x.astype(jnp.float32)).astype(jnp.bfloat16)
    value_x_grad = (mixed_grad * gate_c.astype(jnp.float32)).astype(jnp.bfloat16)
    return (
        w_gate_grad,
        w_up_grad,
        w_down_grad,
        moe_in_grad,
        proj_grad,
        gate_b_grad,
        gate_c_grad,
        value_x_grad,
    )


def solution(mesh):
    in_specs = (
        P("sp", None),
        P("sp", None),
        P("sp", None),
        P("sp", None),
        P("sp", "tp", None),
        P("sp", "tp", None),
        P("sp", "tp", None),
        P("tp", "sp"),
        P("tp", "sp"),
        P("tp", "sp"),
        P(None, "tp"),
        P("tp", None),
    )
    out_specs = (
        P("sp", "tp", None),
        P("sp", "tp", None),
        P("sp", "tp", None),
        P("sp", "tp"),
        P("tp", "sp"),
        P("tp", "sp"),
        P("tp", "sp"),
        P("tp", "sp"),
    )
    return jax.shard_map(
        on_device, mesh=mesh, in_specs=in_specs, out_specs=out_specs, check_vma=False
    )
```

profile of v0, /device:TPU:0, one launch (start us, length us, event | category | flops | bytes accessed | tf_op | source)
XLA Modules:
  0.0 214.4 jit_solution(2672722682063082941)
XLA Ops:
  7.2 0.0 copy-start
  7.2 0.0 all-gather.5.cloned.1.call-start
  7.2 0.9 copy.23
  8.2 0.1 eq.29
  8.3 0.1 eq.25
  8.5 0.7 broadcast_multiply_fusion
  9.2 0.8 reduce-window.6
  10.0 0.2 slice_reduce_fusion
  10.3 0.1 fusion.26
  10.4 0.1 copy.22
  10.5 0.1 mul.125
  10.7 2.9 %scatter_custom_fusion = s32[384]{0:T(512)S(1)} fusion(s32[384]{0:T(512)S(1)} %fusion.30, s32[384]{0:T(512)S(1)} %iota.11, s32[]{:T(128)} %constant.15.clone.1), kind=kCustom, calls=%fused_computation.78 | custom fusion | bytes 1540 | tf_op jit(solution)/shard_map/scatter | solution.py:45
  13.6 1.1 constant_dynamic-slice_fusion
  14.7 2.1 gather_fusion.2
  16.8 18.8 %all_to_all.33 = bf16[8,48,512]{2,1,0:T(8,128)(2,1)} all-to-all(bf16[8,48,512]{2,1,0:T(8,128)(2,1)S(1)} %bitcast.57), channel_id=1, replica_groups=mesh['sp'=8,'tp'=4] {'sp'}, dimensions={0} | all-to-all | bytes 786432 | tf_op jit(solution)/shard_map/all_to_all | solution.py:55
  35.5 0.0 all-gather.5.cloned.1.call-update
  35.6 0.0 all-gather.3.cloned.1.call-start
  35.6 2.1 gather_fusion.1
  37.7 0.1 copy.21
  37.8 0.1 reshape.90
  38.0 2.8 %gather_fusion = f32[384]{0:T(512)S(1)} fusion(f32[384]{0:T(512)S(1)} %reshape.90, s32[1024]{0:T(1024)S(1)} %get-tuple-element.39), kind=kCustom, calls=%fused_computation | custom fusion | bytes 4608 | tf_op jit(solution)/shard_map/gather | solution.py:48
  40.8 0.1 mul.127
  40.8 0.1 fusion.12
  41.0 15.6 %all_to_all.34 = bf16[8,48,512]{2,1,0:T(8,128)(2,1)} all-to-all(bf16[8,48,512]{2,1,0:T(8,128)(2,1)S(1)} %fusion.12), channel_id=1, replica_groups=mesh['sp'=8,'tp'=4] {'sp'}, dimensions={0} | all-to-all | bytes 786432 | tf_op jit(solution)/shard_map/all_to_all | solution.py:56
  56.6 0.0 all-gather.3.cloned.1.call-update
  56.6 0.0 reduce-scatter.3.cloned.1.call-start
  56.7 8.7 %all-gather.5.cloned.1.call-done = bf16[384,2048]{1,0:T(8,128)(2,1)} async-done(((bf16[384,512]{1,0:T(8,128)(2,1)}), bf16[384,2048]{1,0:T(8,128)(2,1)}) %all-gather.5.cloned.1.call-update) | async-done | bytes 1572880 | tf_op jit(solution)/shard_map/all_gather | solution.py:59
  65.4 2.6 %fusion.5 = f32[384,512]{1,0:T(8,128)S(1)} fusion(bf16[384,2048]{1,0:T(8,128)(2,1)} %all-gather.5.cloned.1.call-done, bf16[1,512,2048]{2,1,0:T(8,128)(2,1)S(1)} %copy-done), kind=kOutput, calls=%fused_computation.15 | convolution fusion | flops 805306368 | bytes 4456448 | tf_op jit(solution)/shard_map/dot_general | solution.py:64
  67.9 0.0 copy-done.2
  67.9 0.0 copy-done.14
  68.0 0.0 copy-start.17
  68.0 1.9 fusion.8
  69.9 28.1 %all-gather.3.cloned.1.call-done = bf16[384,2048]{1,0:T(8,128)(2,1)} async-done(((bf16[384,512]{1,0:T(8,128)(2,1)}), bf16[384,2048]{1,0:T(8,128)(2,1)}) %all-gather.3.cloned.1.call-update) | async-done | bytes 1572880 | tf_op jit(solution)/shard_map/all_gather | solution.py:60
  97.9 0.0 copy-done.17
  97.9 3.4 %multiply_convert_fusion.1 = (bf16[384,512]{1,0:T(8,128)(2,1)S(1)}, bf16[384,512]{1,0:T(8,128)(2,1)S(1)}) fusion(f32[384,512]{1,0:T(8,128)S(1)} %fusion.5, f32[384,512]{1,0:T(8,128)} %fusion.8, bf16[384,2048]{1,0:T(8,128)(2,1)} %all-gather.3.cloned.1.call-done, bf16[1,512,2048]{2,1,0:T(8,128)(2,1)} %param.18), kind=kOutput, calls=%fused_computation.27 | convolution fusion | flops 807862272 | bytes 6029312 | tf_op jit(solution)/shard_map/dot_general | solution.py:70
  101.4 0.0 copy-start.3
  101.4 1.0 fusion.3
  102.4 0.9 copy-done.3
  103.3 2.1 add_convert_fusion
  105.4 0.0 reduce-scatter.3.cloned.1.call-update
  105.4 31.3 %reduce-scatter.3.cloned.1.call-done = bf16[384,512]{1,0:T(8,128)(2,1)} async-done(((bf16[384,2048]{1,0:T(8,128)(2,1)}), bf16[384,512]{1,0:T(8,128)(2,1)}) %reduce-scatter.3.cloned.1.call-update) | async-done | bytes 393232 | tf_op jit(solution)/shard_map/reduce_scatter | solution.py:90
  136.7 4.6 %all-to-all-start.2 = ((bf16[8,48,512]{2,1,0:T(8,128)(2,1)}), bf16[8,48,512]{2,1,0:T(8,128)(2,1)S(1)}, u32[]{:S(2)}, u32[]{:S(2)}) async-start(bf16[8,48,512]{2,1,0:T(8,128)(2,1)} %bitcast.58), calls=%async_computation.3 | async-start | bytes 786432 | tf_op jit(solution)/shard_map/all_to_all | solution.py:93
  141.3 0.0 reduce-scatter.5.cloned.1.call-start
  141.4 2.4 %collective-permute-start = (bf16[256,2]{0,1:T(2,128)(2,1)S(1)}, bf16[256,2]{0,1:T(2,128)(2,1)S(1)}, u32[]{:S(2)}, u32[]{:S(2)}) collective-permute-start(bf16[256,2]{0,1:T(2,128)(2,1)S(1)} %slice.60), channel_id=1, source_target_pairs={{0,4},{4,8},{8,12},{12,16},{16,20},{20,24},{24,28},{1,5},{5,9},{9,... | collective-permute-start | bytes 3080 | tf_op jit(solution)/shard_map/ppermute | solution.py:12
  143.8 0.8 collective-permute-done
  144.6 9.2 %all-to-all-done.2 = bf16[8,48,512]{2,1,0:T(8,128)(2,1)S(1)} async-done(((bf16[8,48,512]{2,1,0:T(8,128)(2,1)}), bf16[8,48,512]{2,1,0:T(8,128)(2,1)S(1)}, u32[]{:S(2)}, u32[]{:S(2)}) %all-to-all-start.2) | async-done | bytes 393248 | tf_op jit(solution)/shard_map/all_to_all | solution.py:93
  153.8 2.6 %gather_fusion.3 = bf16[384,512]{1,0:T(8,128)(2,1)} fusion(bf16[384,512]{1,0:T(8,128)(2,1)S(1)} %bitcast.53, s32[1024]{0:T(1024)S(1)} %pad_clamp_fusion), kind=kCustom, calls=%fused_computation.3 | custom fusion | bytes 787968 | tf_op jit(solution)/shard_map/gather | solution.py:94
  156.4 1.1 gather.18
  157.6 1.7 reduce_sum.22
  159.3 11.3 %all_gather.11 = bf16[192,2048]{1,0:T(8,128)(2,1)S(1)} all-gather(bf16[192,512]{1,0:T(8,128)(2,1)} %reduce_sum.22), channel_id=1, replica_groups=mesh['sp'=8,'tp'=4] {'tp'}, dimensions={1}, use_global_device_ids=true | all-gather | bytes 983040 | tf_op jit(solution)/shard_map/all_gather | solution.py:96
  170.6 2.4 %multiply_convert_fusion.4 = (bf16[256,192]{0,1:T(8,128)(2,1)}, f32[256,192]{0,1:T(8,128)S(1)}, f32[256,192]{0,1:T(8,128)S(1)}) fusion(f32[256,194]{0,1:T(8,128)S(1)} %maximum_convert_fusion, f32[256]{0:T(256)S(1)} %bitcast.61, f32[256]{0:T(256)S(1)} %bitcast.63, f32[256]{0:T(256)S(1)} %bitcast.59, bf16[256,192]{0,1:T(8,128)(2,1)} %param.19, ...), kind=kOutput, calls=%fused_computation.54 | convolution fusion | flops 203341824 | bytes 3804160 | tf_op jit(solution)/shard_map/dot_general | solution.py:109
  173.0 1.5 convolution_convert_fusion.3
  174.6 0.0 reduce-scatter.5.cloned.1.call-update
  174.6 0.0 copy-start.19
  174.6 4.3 %fusion.1 = bf16[1,512,2048]{2,1,0:T(8,128)(2,1)} fusion(bf16[384,512]{1,0:T(8,128)(2,1)} %copy-done.4, bf16[384,2048]{1,0:T(8,128)(2,1)} %all-gather.5.cloned.1.call-done), kind=kOutput, calls=%fused_computation.10 | convolution fusion | flops 806354944 | bytes 4063232 | tf_op jit(solution)/shard_map/dot_general | solution.py:80
  178.9 2.7 %fusion.2 = bf16[1,512,2048]{2,1,0:T(8,128)(2,1)} fusion(bf16[384,2048]{1,0:T(8,128)(2,1)S(1)} %copy-done.16, f32[384,512]{1,0:T(8,128)S(1)} %copy-done.19, f32[384,512]{1,0:T(8,128)S(1)} %copy-done.18), kind=kOutput, calls=%fused_computation.11 | convolution fusion | flops 807534592 | bytes 5242880 | tf_op jit(solution)/shard_map/dot_general | solution.py:83
  181.6 1.4 collective-permute-start.1
  183.0 2.6 %fusion = bf16[1,512,2048]{2,1,0:T(8,128)(2,1)} fusion(bf16[384,512]{1,0:T(8,128)(2,1)S(1)} %copy-done.11, bf16[384,2048]{1,0:T(8,128)(2,1)S(1)} %copy-done.15), kind=kOutput, calls=%fused_computation.9 | convolution fusion | flops 806354944 | bytes 4063232 | tf_op jit(solution)/shard_map/dot_general | solution.py:77
  185.6 0.0 collective-permute-done.1
  185.6 0.7 fusion.19
  186.4 0.7 fusion.21
  187.0 19.0 %reduce-scatter.5.cloned.1.call-done = bf16[256,256]{1,0:T(8,128)(2,1)} async-done(((bf16[2048,256]{1,0:T(8,128)(2,1)}), bf16[256,256]{1,0:T(8,128)(2,1)}) %reduce-scatter.5.cloned.1.call-update) | async-done | bytes 131088 | tf_op jit(solution)/shard_map/reduce_scatter | solution.py:112
  206.1 0.9 convert_bitcast_fusion
  207.0 0.8 copy.25
  (45 shorter events, 0.2 us)
Async XLA Ops:
  7.2 58.2 %copy-start = (bf16[1,512,2048]{2,1,0:T(8,128)(2,1)S(1)}, bf16[1,512,2048]{2,1,0:T(8,128)(2,1)}, u32[]{:S(2)}) copy-start(bf16[1,512,2048]{2,1,0:T(8,128)(2,1)} %param.16) | copy-start | bytes 6291460
  7.2 58.2 %all-gather.5.cloned.1.call-start = ((), (), s32[]{:S(2)}) async-start(), calls=%async_computation.6 | async-start | bytes 1966080 | tf_op jit(solution)/shard_map/all_gather | solution.py:59
  35.5 2.2 %copy-start.13 = (f32[192,2]{0,1:T(2,128)S(1)}, f32[192,2]{0,1:T(2,128)}, u32[]{:S(2)}) copy-start(f32[192,2]{0,1:T(2,128)} %param.15) | copy-start | bytes 4612
  35.6 62.4 %all-gather.3.cloned.1.call-start = ((), (), s32[]{:S(2)}) async-start(), calls=%async_computation.5 | async-start | bytes 1966080 | tf_op jit(solution)/shard_map/all_gather | solution.py:60
  56.6 80.1 %reduce-scatter.3.cloned.1.call-start = ((), (), s32[]{:S(2)}) async-start(), calls=%async_computation.7 | async-start | bytes 1966080 | tf_op jit(solution)/shard_map/reduce_scatter | solution.py:90
  65.4 2.6 %copy-start.2 = (bf16[1,512,2048]{2,1,0:T(8,128)(2,1)S(1)}, bf16[1,512,2048]{2,1,0:T(8,128)(2,1)}, u32[]{:S(2)}) copy-start(bf16[1,512,2048]{2,1,0:T(8,128)(2,1)} %param.17) | copy-start | bytes 6291460
  65.4 2.6 %copy-start.14 = (bf16[384,2048]{1,0:T(8,128)(2,1)S(1)}, bf16[384,2048]{1,0:T(8,128)(2,1)}, u32[]{:S(2)}) copy-start(bf16[384,2048]{1,0:T(8,128)(2,1)} %all-gather.5.cloned.1.call-done) | copy-start | bytes 4718596
  68.0 30.0 %copy-start.17 = (f32[384,512]{1,0:T(8,128)}, f32[384,512]{1,0:T(8,128)S(1)}, u32[]{:S(2)}) copy-start(f32[384,512]{1,0:T(8,128)S(1)} %fusion.5) | copy-start | bytes 2359300
  101.4 1.0 copy-start.10
  101.4 1.0 copy-start.4
  101.4 1.9 copy-start.3
  105.4 36.0 %copy-start.6 = (bf16[256,192]{0,1:T(8,128)(2,1)S(1)}, bf16[256,192]{0,1:T(8,128)(2,1)}, u32[]{:S(2)}) copy-start(bf16[256,192]{0,1:T(8,128)(2,1)} %param.20) | copy-start | bytes 294916
  105.4 36.0 %copy-start.8 = (bf16[256,192]{0,1:T(8,128)(2,1)S(1)}, bf16[256,192]{0,1:T(8,128)(2,1)}, u32[]{:S(2)}) copy-start(bf16[256,192]{0,1:T(8,128)(2,1)} %param.21) | copy-start | bytes 294916
  105.4 38.4 %copy-start.12 = (f32[3,256]{1,0:T(4,128)S(1)}, f32[3,256]{1,0:T(4,128)}, u32[]{:S(2)}) copy-start(f32[3,256]{1,0:T(4,128)} %param.22) | copy-start | bytes 9220
  136.7 17.1 %all-to-all-start.2 = ((bf16[8,48,512]{2,1,0:T(8,128)(2,1)}), bf16[8,48,512]{2,1,0:T(8,128)(2,1)S(1)}, u32[]{:S(2)}, u32[]{:S(2)}) async-start(bf16[8,48,512]{2,1,0:T(8,128)(2,1)} %bitcast.58), calls=%async_computation.3 | async-start | bytes 786432 | tf_op jit(solution)/shard_map/all_to_all | solution.py:93
  141.3 64.8 %reduce-scatter.5.cloned.1.call-start = ((), (), s32[]{:S(2)}) async-start(), calls=%async_computation.8 | async-start | bytes 1179648 | tf_op jit(solution)/shard_map/reduce_scatter | solution.py:112
  141.4 3.2 %collective-permute-start = (bf16[256,2]{0,1:T(2,128)(2,1)S(1)}, bf16[256,2]{0,1:T(2,128)(2,1)S(1)}, u32[]{:S(2)}, u32[]{:S(2)}) collective-permute-start(bf16[256,2]{0,1:T(2,128)(2,1)S(1)} %slice.60), channel_id=1, source_target_pairs={{0,4},{4,8},{8,12},{12,16},{16,20},{20,24},{24,28},{1,5},{5,9},{9,... | collective-permute-start | bytes 3080 | tf_op jit(solution)/shard_map/ppermute | solution.py:12
  153.8 16.8 %copy-start.1 = (bf16[192,2048]{1,0:T(8,128)(2,1)S(1)}, bf16[192,2048]{1,0:T(8,128)(2,1)}, u32[]{:S(2)}) copy-start(bf16[192,2048]{1,0:T(8,128)(2,1)} %param.13) | copy-start | bytes 2359300
  159.3 13.7 %copy-start.5 = (bf16[256,192]{0,1:T(8,128)(2,1)S(1)}, bf16[256,192]{0,1:T(8,128)(2,1)}, u32[]{:S(2)}) copy-start(bf16[256,192]{0,1:T(8,128)(2,1)} %param.19) | copy-start | bytes 294916
  174.6 4.3 %copy-start.16 = (bf16[384,2048]{1,0:T(8,128)(2,1)S(1)}, bf16[384,2048]{1,0:T(8,128)(2,1)}, u32[]{:S(2)}) copy-start(bf16[384,2048]{1,0:T(8,128)(2,1)} %all-gather.3.cloned.1.call-done) | copy-start | bytes 4718596
  174.6 4.3 %copy-start.18 = (f32[384,512]{1,0:T(8,128)S(1)}, f32[384,512]{1,0:T(8,128)}, u32[]{:S(2)}) copy-start(f32[384,512]{1,0:T(8,128)} %copy-done.17) | copy-start | bytes 2359300
  174.6 4.3 %copy-start.19 = (f32[384,512]{1,0:T(8,128)S(1)}, f32[384,512]{1,0:T(8,128)}, u32[]{:S(2)}) copy-start(f32[384,512]{1,0:T(8,128)} %fusion.8) | copy-start | bytes 2359300
  178.9 4.1 %copy-start.11 = (bf16[384,512]{1,0:T(8,128)(2,1)S(1)}, bf16[384,512]{1,0:T(8,128)(2,1)}, u32[]{:S(2)}) copy-start(bf16[384,512]{1,0:T(8,128)(2,1)} %copy-done.10) | copy-start | bytes 1179652
  178.9 4.1 %copy-start.15 = (bf16[384,2048]{1,0:T(8,128)(2,1)S(1)}, bf16[384,2048]{1,0:T(8,128)(2,1)}, u32[]{:S(2)}) copy-start(bf16[384,2048]{1,0:T(8,128)(2,1)} %all-gather.5.cloned.1.call-done) | copy-start | bytes 4718596
  181.6 4.1 %copy-start.7 = (bf16[256,192]{0,1:T(8,128)(2,1)S(1)}, bf16[256,192]{0,1:T(8,128)(2,1)}, u32[]{:S(2)}) copy-start(bf16[256,192]{0,1:T(8,128)(2,1)} %param.20) | copy-start | bytes 294916
  181.6 4.8 %copy-start.9 = (bf16[256,192]{0,1:T(8,128)(2,1)S(1)}, bf16[256,192]{0,1:T(8,128)(2,1)}, u32[]{:S(2)}) copy-start(bf16[256,192]{0,1:T(8,128)(2,1)} %param.21) | copy-start | bytes 294916
  181.6 4.1 %collective-permute-start.1 = (f32[256,2]{0,1:T(2,128)S(1)}, f32[256,2]{0,1:T(2,128)S(1)}, u32[]{:S(2)}, u32[]{:S(2)}) collective-permute-start(f32[256,2]{0,1:T(2,128)S(1)} %slice.64), channel_id=1, source_target_pairs={{4,0},{8,4},{12,8},{16,12},{20,16},{24,20},{28,24},{5,1},{9,5},{13... | collective-permute-start | bytes 6152 | tf_op jit(solution)/shard_map/ppermute | solution.py:12
Sparse Core Ops, SparseCore 0:
  35.7 29.6 all-gather.4
  67.2 30.6 all-gather.2
  105.5 31.1 reduce-scatter.2
  174.7 31.3 reduce-scatter.4
where the time goes:
time: 215 us; the launch traced here: 214 us
  waiting for transfers between devices  97.1 us (45%)
  blocking collectives  45.7 us (21%)
  matrix products  24.5 us (11%)
  local copies, waits for them, and re-layouts  18.5 us (9%)
  between operations  14.1 us (7%)
  starting transfers between devices  8.54 us (4%)
  other arithmetic  5.94 us (3%)
    reduce_scatter x1, waiting for transfers between devices, on_device(): lax.psum_scatter(partial_value.astype(jnp.bfloat16), 'tp', scatter_dimens...  31.3 us
    all_gather x1, waiting for transfers between devices, on_device(): lax.all_gather(moved[1], 'tp', axis=1, tiled=True)  28.1 us
    reduce_scatter x1, waiting for transfers between devices, on_device(): lax.psum_scatter(lax.dot_general(stream_grad, mixer_act, (((0,), (1,)), (...  19 us
    all_to_all x1, blocking collectives, on_device(): lax.all_to_all(rows_part, 'sp', split_axis=0, concat_axis=0, tiled=True)  18.8 us
    all_to_all x1, blocking collectives, on_device(): lax.all_to_all(cot_part, 'sp', split_axis=0, concat_axis=0, tiled=True)  15.6 us
    all_gather x1, blocking collectives, on_device(): full_grad = lax.all_gather(moe_in_grad, 'tp', axis=1, tiled=True)  11.3 us
    all_to_all x1, waiting for transfers between devices, on_device(): lax.all_to_all(summed, 'sp', split_axis=0, concat_axis=0, tiled=True)  9.21 us
    all_gather x1, waiting for transfers between devices, on_device(): lax.all_gather(moved[0], 'tp', axis=1, tiled=True)  8.69 us
  transfers between devices with their start and end apart: 7, of which 6 were waited for; matrix products, arithmetic and copies ran while one was open for 10% of the time, Pallas kernels for 0%

commit v1 on v0

--- a/solution.py
+++ b/solution.py
@@ -1,9 +1,307 @@
 import jax
 import jax.numpy as jnp
 from jax import lax
+from jax.experimental import pallas as pl
+from jax.experimental.pallas import tpu as pltpu
 from jax.sharding import PartitionSpec as P
 
 TAPS = 3
+GROUPS = 4
+CORES = 2
+MESH = pl.DeviceIdType.MESH
+
+
+def place():
+    s, t = lax.axis_index("sp"), lax.axis_index("tp")
+    z, c = lax.div(s, CORES), lax.rem(s, CORES)
+    x, y = lax.rem(t, 2), lax.div(t, 2)
+    lanes = (t + 1 - 2 * x, t + 2 - 4 * y, 3 - t)
+    return s, t, z, c, lanes
+
+
+def greet(targets):
+    barrier = pltpu.get_barrier_semaphore()
+    for target in targets:
+        pl.semaphore_signal(barrier, inc=1, device_id=target, device_id_type=MESH)
+    pl.semaphore_wait(barrier, len(targets))
+
+
+def span(index, width):
+    return pl.ds(pl.multiple_of(index * width, width), width)
+
+
+def remote(src, dst, send_sem, recv_sem, target):
+    return pltpu.make_async_remote_copy(
+        src_ref=src,
+        dst_ref=dst,
+        send_sem=send_sem,
+        recv_sem=recv_sem,
+        device_id=target,
+        device_id_type=MESH,
+    )
+
+
+def dispatch_kernel(
+    rows_ref, weight_ref, out_ref, weight_out, s1, r1, s2, r2, s3, r3, sw, rw, sp_, rp_, own
+):
+    s, t, z, c, lanes = place()
+    width = rows_ref.shape[-1] // 4
+    mate = (CORES * z + 1 - c, t)
+    ahead = [lax.rem(z + d, GROUPS) for d in range(GROUPS)]
+    behind = [lax.rem(z + GROUPS - d, GROUPS) for d in range(GROUPS)]
+    greet(
+        [(CORES * ahead[d] + c, t) for d in range(1, GROUPS)]
+        + [(CORES * ahead[d] + 1 - c, t) for d in range(1, GROUPS)]
+        + [(s, lanes[0]), (s, lanes[1]), mate]
+    )
+    quarters = (t, lanes[2])
+    first = {}
+    small = []
+    for d in (2, 1, 3):
+        for j in range(2):
+            cols = span(quarters[j], width)
+            copy = remote(
+                rows_ref.at[ahead[d], :, :, cols],
+                out_ref.at[:, s, :, cols],
+                s1.at[j, d - 1],
+                r1.at[j, d - 1],
+                (CORES * ahead[d] + c, t),
+            )
+            copy.start()
+            first[j, d] = copy
+        for k in range(2):
+            core = c if k == 0 else 1 - c
+            copy = remote(
+                weight_ref.at[ahead[d]],
+                weight_out.at[s],
+                sw.at[k, d - 1],
+                rw.at[k, d - 1],
+                (CORES * ahead[d] + core, t),
+            )
+            copy.start()
+            small.append(copy)
+    pair = [
+        remote(rows_ref.at[z], out_ref.at[:, s], sp_.at[0], rp_.at[0], mate),
+        remote(weight_ref.at[z], weight_out.at[s], sp_.at[1], rp_.at[1], mate),
+    ]
+    local = [
+        pltpu.make_async_copy(rows_ref.at[z], out_ref.at[:, s], own.at[0]),
+        pltpu.make_async_copy(weight_ref.at[z], weight_out.at[s], own.at[1]),
+    ]
+    for copy in pair + local:
+        copy.start()
+    order = (1, 3, 2)
+    second = {}
+    for d in order:
+        first[0, d].wait_recv()
+        cols = span(t, width)
+        block = out_ref.at[:, CORES * behind[d] + c, :, cols]
+        for j in range(2):
+            copy = remote(block, block, s2.at[j, d - 1], r2.at[j, d - 1], (s, lanes[j]))
+            copy.start()
+            second[j, d] = copy
+    third = []
+    for d in order:
+        first[1, d].wait_recv()
+        second[0, d].wait_recv()
+        second[1, d].wait_recv()
+        block = out_ref.at[:, CORES * behind[d] + c]
+        copy = remote(block, block, s3.at[d - 1], r3.at[d - 1], mate)
+        copy.start()
+        third.append(copy)
+    for copy in local:
+        copy.wait()
+    for copy in small + pair + third:
+        copy.wait()
+    for copy in list(first.values()) + list(second.values()):
+        copy.wait_send()
+
+
+def dispatch(rows, weights):
+    groups, two, cap, model = rows.shape
+    vmem = pl.BlockSpec(memory_space=pltpu.VMEM)
+    dma = pltpu.SemaphoreType.DMA
+    return pl.pallas_call(
+        dispatch_kernel,
+        out_shape=(
+            jax.ShapeDtypeStruct((two, CORES * groups, cap, model), rows.dtype),
+            jax.ShapeDtypeStruct((CORES * groups,) + weights.shape[1:], weights.dtype),
+        ),
+        in_specs=[vmem, vmem],
+        out_specs=(vmem, vmem),
+        scratch_shapes=[
+            dma((2, groups - 1)),
+            dma((2, groups - 1)),
+            dma((2, groups - 1)),
+            dma((2, groups - 1)),
+            dma((groups - 1,)),
+            dma((groups - 1,)),
+            dma((2, groups - 1)),
+            dma((2, groups - 1)),
+            dma((2,)),
+            dma((2,)),
+            dma((2,)),
+        ],
+        compiler_params=pltpu.CompilerParams(collective_id=0, has_side_effects=True),
+        name="dispatch",
+    )(rows, weights)
+
+
+def combine_kernel(part_ref, out_ref, mate_in, total, lane_in, done, sa, ra, sb, rb, sc, rc, sd, rd):
+    s, t, z, c, lanes = place()
+    width = part_ref.shape[-1] // 4
+    mate = (CORES * z + 1 - c, t)
+    ahead = [lax.rem(z + d, GROUPS) for d in range(GROUPS)]
+    behind = [lax.rem(z + GROUPS - d, GROUPS) for d in range(GROUPS)]
+    greet(
+        [(CORES * ahead[d] + c, t) for d in range(1, GROUPS)]
+        + [(s, lane) for lane in lanes]
+        + [mate]
+    )
+    order = (2, 1, 3, 0)
+    mine = span(t, width)
+    swap = {}
+    for d in order:
+        swap[d] = remote(part_ref.at[ahead[d], 1 - c], mate_in.at[d], sa.at[d], ra.at[d], mate)
+        swap[d].start()
+    across = {}
+    for d in order:
+        swap[d].wait_recv()
+        total[d] = (
+            part_ref[ahead[d], c].astype(jnp.float32) + mate_in[d].astype(jnp.float32)
+        ).astype(total.dtype)
+        for j in (2, 0, 1):
+            across[j, d] = remote(
+                total.at[d, :, span(lanes[j], width)],
+                lane_in.at[j, d],
+                sb.at[j, d],
+                rb.at[j, d],
+                (s, lanes[j]),
+            )
+            across[j, d].start()
+    home = {}
+    for d in order:
+        value = total[d, :, mine].astype(jnp.float32)
+        for j in range(3):
+            across[j, d].wait_recv()
+            value = value + lane_in[j, d].astype(jnp.float32)
+        value = value.astype(out_ref.dtype)
+        if d == 0:
+            out_ref[z, :, mine] = value
+        else:
+            done[d - 1] = value
+            home[d] = remote(
+                done.at[d - 1],
+                out_ref.at[z, :, mine],
+                sc.at[d - 1],
+                rc.at[d - 1],
+                (CORES * ahead[d] + c, t),
+            )
+            home[d].start()
+    spread = []
+    for d in (0, 1, 3, 2):
+        if d:
+            home[d].wait_recv()
+        block = out_ref.at[behind[d], :, mine]
+        for j in (2, 0, 1):
+            copy = remote(block, block, sd.at[j, d], rd.at[j, d], (s, lanes[j]))
+            copy.start()
+            spread.append(copy)
+    for copy in spread:
+        copy.wait()
+    for copy in list(swap.values()) + list(across.values()) + list(home.values()):
+        copy.wait_send()
+
+
+def combine(part):
+    groups, cores, cap, model = part.shape
+    vmem = pl.BlockSpec(memory_space=pltpu.VMEM)
+    dma = pltpu.SemaphoreType.DMA
+    width = model // 4
+    return pl.pallas_call(
+        combine_kernel,
+        out_shape=jax.ShapeDtypeStruct((groups, cap, model), part.dtype),
+        in_specs=[vmem],
+        out_specs=vmem,
+        scratch_shapes=[
+            pltpu.VMEM((groups, cap, model), part.dtype),
+            pltpu.VMEM((groups, cap, model), part.dtype),
+            pltpu.VMEM((3, groups, cap, width), part.dtype),
+            pltpu.VMEM((groups - 1, cap, width), part.dtype),
+            dma((groups,)),
+            dma((groups,)),
+            dma((3, groups)),
+            dma((3, groups)),
+            dma((groups - 1,)),
+            dma((groups - 1,)),
+            dma((3, groups)),
+            dma((3, groups)),
+        ],
+        compiler_params=pltpu.CompilerParams(collective_id=1, has_side_effects=True),
+        name="combine",
+    )(part)
+
+
+def project_kernel(part_ref, out_ref, mate_in, total, far_in, sa, ra, sb, rb):
+    s, t, z, c, lanes = place()
+    width = out_ref.shape[1]
+    mate = (CORES * z + 1 - c, t)
+    ahead = [lax.rem(z + d, GROUPS) for d in range(GROUPS)]
+    greet([(CORES * ahead[d] + c, t) for d in range(1, GROUPS)] + [mate])
+    order = (2, 1, 3, 0)
+    swap = {}
+    for d in order:
+        cols = span(CORES * ahead[d] + 1 - c, width)
+        swap[d] = remote(part_ref.at[:, cols], mate_in.at[d], sa.at[d], ra.at[d], mate)
+        swap[d].start()
+    far = {}
+    for d in order:
+        swap[d].wait_recv()
+        cols = span(CORES * ahead[d] + c, width)
+        value = part_ref[:, cols].astype(jnp.float32) + mate_in[d].astype(jnp.float32)
+        if d == 0:
+            out_ref[...] = value
+        else:
+            total[d - 1] = value.astype(total.dtype)
+            far[d] = remote(
+                total.at[d - 1],
+                far_in.at[d - 1],
+                sb.at[d - 1],
+                rb.at[d - 1],
+                (CORES * ahead[d] + c, t),
+            )
+            far[d].start()
+    for d in range(1, GROUPS):
+        far[d].wait_recv()
+    out_ref[...] += (
+        far_in[0].astype(jnp.float32) + far_in[1].astype(jnp.float32)
+    ) + far_in[2].astype(jnp.float32)
+    for copy in list(swap.values()) + list(far.values()):
+        copy.wait_send()
+
+
+def project(part):
+    channels, model = part.shape
+    width = model // (CORES * GROUPS)
+    vmem = pl.BlockSpec(memory_space=pltpu.VMEM)
+    dma = pltpu.SemaphoreType.DMA
+    return pl.pallas_call(
+        project_kernel,
+        out_shape=jax.ShapeDtypeStruct((channels, width), jnp.float32),
+        in_specs=[vmem],
+        out_specs=vmem,
+        scratch_shapes=[
+            pltpu.VMEM((GROUPS, channels, width), part.dtype),
+            pltpu.VMEM((GROUPS - 1, channels, width), part.dtype),
+            pltpu.VMEM((GROUPS - 1, channels, width), part.dtype),
+            dma((GROUPS,)),
+            dma((GROUPS,)),
+            dma((GROUPS - 1,)),
+            dma((GROUPS - 1,)),
+        ],
+        compiler_params=pltpu.CompilerParams(collective_id=2, has_side_effects=True),
+        name="project",
+    )(part)
 
 
 def from_behind(array, axis, by):
@@ -12,7 +310,7 @@
     return lax.ppermute(array, axis, pairs)
 
 
-def on_device(
+def on_device_general(
     moe_in,
     cotangent,
     routing,
@@ -142,6 +440,146 @@
     )
 
 
+def on_device_paired(
+    moe_in,
+    cotangent,
+    routing,
+    route_weight,
+    w_gate,
+    w_up,
+    w_down,
+    gate_b,
+    gate_c,
+    value_x,
+    conv_taps,
+    out_proj,
+):
+    tok_rows = routing.shape[0]
+    lane_count = lax.axis_size("tp")
+    model_width = moe_in.shape[1]
+    cap = tok_rows // GROUPS
+    core = lax.rem(lax.axis_index("sp"), CORES)
+    group = routing[:, 0] // CORES
+    at = jnp.arange(tok_rows, dtype=jnp.int32)
+    same = (group[:, None] == group[None, :]) & (at[:, None] < at[None, :])
+    position = group * cap + jnp.sum(same.astype(jnp.int32), axis=0)
+    select = position[None, :] == at[:, None]
+    permute = select.astype(jnp.bfloat16)
+    is_even = routing[:, 0] % CORES == 0
+    by_core = jnp.stack(
+        [
+            jnp.where(is_even, route_weight[:, 0], route_weight[:, 1]),
+            jnp.where(is_even, route_weight[:, 1], route_weight[:, 0]),
+        ]
+    )
+    weights = jnp.sum(jnp.where(select[None], by_core[:, None, :], 0.0), axis=2)
+    weights = weights.reshape(CORES, GROUPS, cap).transpose(1, 0, 2)
+    weights = jnp.pad(weights, ((0, 0), (0, 8 - CORES), (0, 128 - cap)))
+    rows = jnp.stack(
+        [
+            jnp.dot(permute, array, preferred_element_type=jnp.float32)
+            .astype(jnp.bfloat16)
+            .reshape(GROUPS, cap, model_width)
+            for array in (moe_in, cotangent)
+        ],
+        axis=1,
+    )
+    landed, landed_weights = dispatch(rows, weights)
+    arrived = landed[0].reshape(-1, model_width)
+    scales = lax.dynamic_index_in_dim(landed_weights, core, 1, False)[:, :cap].reshape(-1, 1)
+    arrived_cot = (scales * landed[1].reshape(-1, model_width).astype(jnp.float32)).astype(
+        jnp.bfloat16
+    )
+    contract_model = (((1,), (1,)), ((), ()))
+    over_rows = (((0,), (0,)), ((), ()))
+    gate_pre = lax.dot_general(
+        arrived, w_gate[0], contract_model, preferred_element_type=jnp.float32
+    )
+    up_pre = lax.dot_general(arrived, w_up[0], contract_model, preferred_element_type=jnp.float32)
+    sigmoid_gate = jax.nn.sigmoid(gate_pre)
+    hidden = (gate_pre * sigmoid_gate * up_pre).astype(jnp.bfloat16)
+    hidden_grad = lax.dot_general(
+        arrived_cot, w_down[0], contract_model, preferred_element_type=jnp.float32
+    )
+    gate_grad = (
+        hidden_grad * up_pre * sigmoid_gate * (1.0 + gate_pre * (1.0 - sigmoid_gate))
+    ).astype(jnp.bfloat16)
+    up_grad = (hidden_grad * gate_pre * sigmoid_gate).astype(jnp.bfloat16)
+    w_gate_grad = lax.dot_general(
+        gate_grad, arrived, over_rows, preferred_element_type=jnp.float32
+    ).astype(jnp.bfloat16)[None]
+    w_up_grad = lax.dot_general(
+        up_grad, arrived, over_rows, preferred_element_type=jnp.float32
+    ).astype(jnp.bfloat16)[None]
+    w_down_grad = lax.dot_general(
+        hidden, arrived_cot, over_rows, preferred_element_type=jnp.float32
+    ).astype(jnp.bfloat16)[None]
+    partial_value = jnp.dot(gate_grad, w_gate[0], preferred_element_type=jnp.float32) + jnp.dot(
+        up_grad, w_up[0], preferred_element_type=jnp.float32
+    )
+    summed = combine(
+        partial_value.astype(jnp.bfloat16).reshape(GROUPS, CORES, cap, model_width)
+    )
+    full_grad = lax.dot_general(
+        permute,
+        summed.reshape(tok_rows, model_width),
+        over_rows,
+        preferred_element_type=jnp.float32,
+    ).astype(jnp.bfloat16)
+    col_width = model_width // lane_count
+    moe_in_grad = lax.dynamic_slice_in_dim(
+        full_grad, lax.axis_index("tp") * col_width, col_width, 1
+    )
+    stream_grad = (cotangent.astype(jnp.float32) + full_grad.astype(jnp.float32)).astype(
+        jnp.bfloat16
+    )
+    mixed_in = lax.optimization_barrier(
+        (gate_c.astype(jnp.float32) * value_x.astype(jnp.float32)).astype(jnp.bfloat16)
+    )
+    earlier = from_behind(mixed_in[:, tok_rows - (TAPS - 1) :], "sp", 1)
+    extended = jnp.concatenate([earlier, mixed_in], axis=1).astype(jnp.float32)
+    conv_out = jnp.zeros(mixed_in.shape, jnp.float32)
+    for tap in range(TAPS):
+        conv_out = conv_out + conv_taps[tap][:, None] * extended[:, tap : tap + tok_rows]
+    mixer_act = (gate_b.astype(jnp.float32) * conv_out).astype(jnp.bfloat16)
+    act_grad = lax.dot_general(
+        out_proj, stream_grad, contract_model, preferred_element_type=jnp.float32
+    )
+    proj_grad = project(
+        jnp.dot(mixer_act, stream_grad, preferred_element_type=jnp.float32).astype(jnp.bfloat16)
+    )
+    gate_b_grad = (act_grad * conv_out).astype(jnp.bfloat16)
+    conv_grad = act_grad * gate_b.astype(jnp.float32)
+    later = from_behind(conv_grad[:, : TAPS - 1], "sp", -1)
+    extended_grad = jnp.concatenate([conv_grad, later], axis=1)
+    mixed_grad = jnp.zeros(conv_grad.shape, jnp.float32)
+    for tap in range(TAPS):
+        offset = TAPS - 1 - tap
+        mixed_grad = (
+            mixed_grad + conv_taps[tap][:, None] * extended_grad[:, offset : offset + tok_rows]
+        )
+    gate_c_grad = (mixed_grad * value_x.astype(jnp.float32)).astype(jnp.bfloat16)
+    value_x_grad = (mixed_grad * gate_c.astype(jnp.float32)).astype(jnp.bfloat16)
+    return (
+        w_gate_grad,
+        w_up_grad,
+        w_down_grad,
+        moe_in_grad,
+        proj_grad,
+        gate_b_grad,
+        gate_c_grad,
+        value_x_grad,
+    )
+
+
+def on_device(*args):
+    routes = args[2].shape[1]
+    experts, lane_count = lax.axis_size("sp"), lax.axis_size("tp")
+    if experts == CORES * GROUPS and routes == CORES and lane_count == 4:
+        return on_device_paired(*args)
+    return on_device_general(*args)
+
+
 def solution(mesh):
     in_specs = (
         P("sp", None),

time: 215 us -> 127 us (0.59)
  waiting for transfers between devices: 97.1 us -> 0.01 us
  Pallas kernels: 0 us -> 78.4 us
  blocking collectives: 45.7 us -> 0 us
  local copies, waits for them, and re-layouts: 18.5 us -> 5.03 us
  between operations: 14.1 us -> 0.96 us
  other arithmetic: 5.94 us -> 13.8 us
  starting transfers between devices: 8.54 us -> 3.68 us
    pallas_call x0 -> x3, Pallas kernels: none -> 78.4 us  [the longest x1 34.7 us: combine(): pl.pallas_call(combine_kernel, out_shape=jax.ShapeDtypeStruct((groups, ca...]
    reduce_scatter x2 -> x0, waiting for transfers between devices: 50.3 us -> none  [the longest x1 31.3 us: on_device(): lax.psum_scatter(partial_value.astype(jnp.bfloat16), 'tp', scatter_dimens...]
    all_gather x2 -> x0, waiting for transfers between devices: 36.8 us -> none  [the longest x1 28.1 us: on_device(): lax.all_gather(moved[1], 'tp', axis=1, tiled=True)]
    all_to_all x2 -> x0, blocking collectives: 34.4 us -> none  [the longest x1 18.8 us: on_device(): lax.all_to_all(rows_part, 'sp', split_axis=0, concat_axis=0, tiled=True)]
    all_gather x1 -> x0, blocking collectives: 11.3 us -> none  [on_device(): full_grad = lax.all_gather(moe_in_grad, 'tp', axis=1, tiled=True)]
    gather x5 -> x0, local copies, waits for them, and re-layouts: 10.6 us -> none  [the longest x2 3.72 us: on_device(): per_route = returned[slot_index].astype(jnp.float32)]
    all_to_all x1 -> x0, waiting for transfers between devices: 9.21 us -> none  [on_device(): lax.all_to_all(summed, 'sp', split_axis=0, concat_axis=0, tiled=True)]
    convert_element_type x6 -> x7, other arithmetic: 1.59 us -> 10.3 us  [the longest x1 4.67 us: on_device_paired(): landed[1].reshape(-1, model_width).astype(jnp.float32)]
  transfers between devices with their start and end apart: 7 -> 2, of which waited for: 6 -> 0; matrix products, arithmetic and copies ran while one was open for 10% -> 28% of each run, Pallas kernels for 0% -> 62%
where the time goes in v1:
time: 127 us; the launch traced here: 126 us
  Pallas kernels  78.4 us (62%)
  matrix products  24.4 us (19%)
  other arithmetic  13.8 us (11%)
  local copies, waits for them, and re-layouts  5.03 us (4%)
  starting transfers between devices  3.68 us (3%)
    pallas_call x1, Pallas kernels, combine(): pl.pallas_call(combine_kernel, out_shape=jax.ShapeDtypeStruct((groups, ca...  34.7 us
    pallas_call x1, Pallas kernels, dispatch(): pl.pallas_call(dispatch_kernel, out_shape=(jax.ShapeDtypeStruct((two, COR...  27 us
    pallas_call x1, Pallas kernels, project(): pl.pallas_call(project_kernel, out_shape=jax.ShapeDtypeStruct((channels,...  16.7 us
    convert_element_type x1, other arithmetic, on_device_paired(): landed[1].reshape(-1, model_width).astype(jnp.float32)  4.67 us
    ppermute x2, starting transfers between devices, from_behind(): return lax.ppermute(array, axis, pairs)  3.68 us
    convert_element_type x2, other arithmetic, on_device_paired(): (scales * landed[1].reshape(-1, model_width).astype(jnp.float32)).astype(...  3.1 us
    unnamed x29, local copies, waits for them, and re-layouts  2.78 us
    dot_general x2, matrix products, on_device_paired(): jnp.dot(permute, array, preferred_element_type=jnp.float32)  2.75 us
  transfers between devices with their start and end apart: 2, of which 0 were waited for; matrix products, arithmetic and copies ran while one was open for 28% of the time, Pallas kernels for 62%

profile of v1, /device:TPU:0, one launch (start us, length us, event | category | flops | bytes accessed | tf_op | source)
XLA Modules:
  0.0 126.2 jit_solution(17284875374082213757)
XLA Ops:
  0.6 0.0 copy-start
  0.6 0.0 copy-start.12
  0.7 0.0 copy-start.6
  0.7 0.0 copy-start.10
  0.7 1.1 fusion.20
  1.8 2.4 %collective-permute-start = (bf16[256,2]{0,1:T(2,128)(2,1)S(1)}, bf16[256,2]{0,1:T(2,128)(2,1)S(1)}, u32[]{:S(2)}, u32[]{:S(2)}) collective-permute-start(bf16[256,2]{0,1:T(2,128)(2,1)S(1)} %slice.70), channel_id=1, source_target_pairs={{0,4},{4,8},{8,12},{12,16},{16,20},{20,24},{24,28},{1,5},{5,9},{9,... | collective-permute-start | bytes 3080 | tf_op jit(solution)/shard_map/ppermute | solution.py:310
  4.2 0.7 and_select_fusion.1
  5.0 0.1 convert_reduce_fusion
  5.1 1.5 %convolution_convert_fusion.5 = bf16[192,2048]{1,0:T(8,128)(2,1)S(1)} fusion(bf16[192,2048]{1,0:T(8,128)(2,1)} %param.13, s32[192]{0:T(256)S(1)} %multiply_add_fusion), kind=kOutput, calls=%fused_computation.12 | convolution fusion | flops 151425024 | bytes 1573632 | tf_op jit(solution)/shard_map/dot_general | solution.py:480
  6.6 0.0 copy-done.6
  6.6 1.2 convolution_convert_fusion.6
  7.9 0.0 copy-done.12
  7.9 0.0 copy-done.10
  7.9 0.2 select_reduce_fusion
  8.1 0.1 reshape.199
  8.2 2.4 %pad_maximum_fusion.rows_ref = bf16[4,2,48,2048]{3,2,1,0:T(8,128)(2,1)} fusion(bf16[4,1,48,2048]{3,2,1,0:T(8,128)(2,1)S(1)} %bitcast.67, bf16[4,1,48,2048]{3,2,1,0:T(8,128)(2,1)} %bitcast.68), kind=kLoop, calls=%fused_computation.23 | loop fusion | flops 786432 | bytes 3145728 | tf_op jit(solution)/shard_map/stack | solution.py:478
  10.6 0.6 pad.4.weight_ref
  11.2 27.0 %dispatch.1 = (bf16[2,8,48,2048]{3,2,1,0:T(8,128)(2,1)}, f32[8,8,128]{2,1,0:T(8,128)}) custom-call(bf16[4,2,48,2048]{3,2,1,0:T(8,128)(2,1)} %pad_maximum_fusion.rows_ref, f32[4,8,128]{2,1,0:T(8,128)} %pad.4.weight_ref), custom_call_target="tpu_custom_call" | custom-call | tf_op jit(solution)/shard_map/dispatch/pallas_call | solution.py:124
  38.2 4.7 %slice_convert_fusion = (f32[1,8,48,2048]{3,2,1,0:T(8,128)}, bf16[1,8,48,2048]{3,2,1,0:T(8,128)(2,1)}) fusion(bf16[2,8,48,2048]{3,2,1,0:T(8,128)(2,1)} %get-tuple-element.11), kind=kLoop, calls=%fused_computation.25 | loop fusion | flops 786432 | bytes 7864320 | tf_op jit(solution)/shard_map/convert_element_type | solution.py:490
  42.9 0.8 constant_dynamic-slice_fusion.1
  43.7 2.9 %multiply_convert_fusion = bf16[1,8,48,2048]{3,2,1,0:T(8,128)(2,1)} fusion(f32[8,48]{1,0:T(8,128)S(1)} %bitcast.75, bf16[2,8,48,2048]{3,2,1,0:T(8,128)(2,1)} %get-tuple-element.11), kind=kLoop, calls=%fused_computation.3 | loop fusion | flops 2359296 | bytes 3147264 | tf_op jit(solution)/shard_map/convert_element_type | solution.py:490
  46.5 0.1 mul.130
  46.6 0.0 copy-done
  46.6 0.0 copy-start.3
  46.6 0.0 copy-start.5
  46.6 2.6 %fusion.6 = f32[384,512]{1,0:T(8,128)S(1)} fusion(bf16[384,2048]{1,0:T(8,128)(2,1)} %bitcast.71, bf16[1,512,2048]{2,1,0:T(8,128)(2,1)S(1)} %copy-done), kind=kOutput, calls=%fused_computation.16 | convolution fusion | flops 805306368 | bytes 4456448 | tf_op jit(solution)/shard_map/dot_general | solution.py:495
  49.2 0.0 copy-done.3
  49.2 0.0 copy-done.5
  49.2 0.0 copy-start.4
  49.3 0.0 copy-start.13
  49.3 1.0 fusion.9
  50.3 0.4 copy-done.4
  50.7 0.7 copy-done.13
  51.3 1.3 %multiply_convert_fusion.2 = (bf16[384,512]{1,0:T(8,128)(2,1)S(1)}, bf16[384,512]{1,0:T(8,128)(2,1)S(1)}) fusion(f32[384,512]{1,0:T(8,128)S(1)} %fusion.6, f32[384,512]{1,0:T(8,128)S(1)} %fusion.9, bf16[384,2048]{1,0:T(8,128)(2,1)S(1)} %bitcast.70, bf16[1,512,2048]{2,1,0:T(8,128)(2,1)S(1)} %copy-done.13), kind=kOutput, calls=%fused_computation.28 | convolution fusion | flops 807862272 | bytes 6029312 | tf_op jit(solution)/shard_map/dot_general | solution.py:501
  52.7 2.6 %fusion.1 = bf16[1,512,2048]{2,1,0:T(8,128)(2,1)} fusion(bf16[384,512]{1,0:T(8,128)(2,1)S(1)} %get-tuple-element.21, bf16[384,2048]{1,0:T(8,128)(2,1)S(1)} %bitcast.73), kind=kOutput, calls=%fused_computation.7 | convolution fusion | flops 806354944 | bytes 4063232 | tf_op jit(solution)/shard_map/dot_general | solution.py:508
  55.3 1.0 fusion.4
  56.3 0.0 copy-start.1
  56.3 2.6 %fusion.2 = bf16[1,512,2048]{2,1,0:T(8,128)(2,1)} fusion(bf16[384,512]{1,0:T(8,128)(2,1)S(1)} %get-tuple-element.20, bf16[384,2048]{1,0:T(8,128)(2,1)S(1)} %bitcast.74), kind=kOutput, calls=%fused_computation.8 | convolution fusion | flops 806354944 | bytes 4063232 | tf_op jit(solution)/shard_map/dot_general | solution.py:511
  58.9 0.0 copy-done.1
  58.9 0.2 fusion
  59.2 2.7 %fusion.3 = bf16[1,512,2048]{2,1,0:T(8,128)(2,1)} fusion(bf16[384,2048]{1,0:T(8,128)(2,1)S(1)} %fusion, f32[384,512]{1,0:T(8,128)S(1)} %fusion.9, f32[384,512]{1,0:T(8,128)S(1)} %fusion.6), kind=kOutput, calls=%fused_computation.9 | convolution fusion | flops 807534592 | bytes 5242880 | tf_op jit(solution)/shard_map/dot_general | solution.py:514
  61.8 2.2 %add_convert_fusion = bf16[384,2048]{1,0:T(8,128)(2,1)} fusion(f32[384,2048]{1,0:T(8,128)S(1)} %fusion.4, bf16[384,512]{1,0:T(8,128)(2,1)S(1)} %get-tuple-element.20, bf16[1,512,2048]{2,1,0:T(8,128)(2,1)S(1)} %copy-done.3), kind=kOutput, calls=%fused_computation.2 | convolution fusion | flops 806879232 | bytes 7208960 | tf_op jit(solution)/shard_map/dot_general | solution.py:517
  64.0 0.0 copy-start.11
  64.0 0.0 copy-start.7
  64.0 34.7 %combine.1 = bf16[4,48,2048]{2,1,0:T(8,128)(2,1)} custom-call(bf16[4,2,48,2048]{3,2,1,0:T(8,128)(2,1)} %bitcast.66), custom_call_target="tpu_custom_call" | custom-call | tf_op jit(solution)/shard_map/combine/pallas_call | solution.py:221
  98.7 1.6 %convolution_convert_fusion.4 = bf16[192,2048]{1,0:T(8,128)(2,1)S(1)} fusion(bf16[192,2048]{1,0:T(8,128)(2,1)} %bitcast.69, s32[192]{0:T(256)S(1)} %multiply_add_fusion), kind=kOutput, calls=%fused_computation.11 | convolution fusion | flops 151425024 | bytes 1573632 | tf_op jit(solution)/shard_map/dot_general | solution.py:523
  100.2 0.0 copy-done.11
  100.2 0.0 copy-start.2
  100.3 0.7 constant_dynamic-slice_fusion
  101.0 0.0 collective-permute-done
  101.0 0.0 copy-done.7
  101.0 2.6 %multiply_convert_fusion.5 = (bf16[256,192]{0,1:T(8,128)(2,1)}, f32[256,192]{0,1:T(8,128)S(1)}, f32[256,192]{0,1:T(8,128)S(1)}) fusion(f32[256,194]{0,1:T(8,128)S(1)} %maximum_convert_fusion, f32[256]{0:T(256)S(1)} %bitcast.80, f32[256]{0:T(256)S(1)} %bitcast.82, f32[256]{0:T(256)S(1)} %bitcast.78, bf16[256,192]{0,1:T(8,128)(2,1)S(1)} %copy-done.7, ...), kind=kOutput, calls=%fused_computation.55 | convolution fusion | flops 203341824 | bytes 3804160 | tf_op jit(solution)/shard_map/dot_general | solution.py:545
  103.6 1.3 %collective-permute-start.1 = (f32[256,2]{0,1:T(2,128)S(1)}, f32[256,2]{0,1:T(2,128)S(1)}, u32[]{:S(2)}, u32[]{:S(2)}) collective-permute-start(f32[256,2]{0,1:T(2,128)S(1)} %slice.74), channel_id=1, source_target_pairs={{4,0},{8,4},{12,8},{16,12},{20,16},{24,20},{28,24},{5,1},{9,5},{13... | collective-permute-start | bytes 6152 | tf_op jit(solution)/shard_map/ppermute | solution.py:310
  104.9 0.0 copy-done.2
  104.9 0.0 copy-start.8
  104.9 0.0 copy-start.9
  104.9 1.5 %convolution_convert_fusion.3.part_ref = bf16[256,2048]{1,0:T(8,128)(2,1)} fusion(bf16[192,2048]{1,0:T(8,128)(2,1)S(1)} %convolution_convert_fusion.4, bf16[192,2048]{1,0:T(8,128)(2,1)S(1)} %copy-done.2, f32[256,192]{0,1:T(8,128)S(1)} %get-tuple-element.15, bf16[256,192]{0,1:T(8,128)(2,1)S(1)} %copy-done.7), kind=kOutput, calls=%fused_computation.10 | convolution fusion | flops 203571200 | bytes 2916352 | tf_op jit(solution)/shard_map/dot_general | solution.py:549
  106.4 16.7 %project.1 = f32[256,256]{1,0:T(8,128)} custom-call(bf16[256,2048]{1,0:T(8,128)(2,1)} %convolution_convert_fusion.3.part_ref), custom_call_target="tpu_custom_call" | custom-call | tf_op jit(solution)/shard_map/project/pallas_call | solution.py:288
  123.1 0.0 collective-permute-done.1
  123.1 0.0 copy-done.8
  123.2 0.7 fusion.19
  123.9 0.0 copy-done.9
  123.9 0.7 fusion.21
  124.5 1.7 %copy.25 = f32[256,256]{1,0:T(8,128)} copy(f32[256,256]{1,0:T(8,128)} %project.1) | data formatting | bytes 524288
  (11 shorter events, 0.1 us)
Async XLA Ops:
  0.6 46.0 %copy-start = (bf16[1,512,2048]{2,1,0:T(8,128)(2,1)S(1)}, bf16[1,512,2048]{2,1,0:T(8,128)(2,1)}, u32[]{:S(2)}) copy-start(bf16[1,512,2048]{2,1,0:T(8,128)(2,1)} %param.16) | copy-start | bytes 6291460
  0.6 7.2 %copy-start.12 = (s32[192,2]{0,1:T(2,128)S(1)}, s32[192,2]{0,1:T(2,128)}, u32[]{:S(2)}) copy-start(s32[192,2]{0,1:T(2,128)} %param.14) | copy-start | bytes 4612
  0.7 6.0 %copy-start.6 = (bf16[192,2048]{1,0:T(8,128)(2,1)S(1)}, bf16[192,2048]{1,0:T(8,128)(2,1)}, u32[]{:S(2)}) copy-start(bf16[192,2048]{1,0:T(8,128)(2,1)} %param.12) | copy-start | bytes 2359300
  0.7 7.2 %copy-start.10 = (f32[192,2]{0,1:T(2,128)S(1)}, f32[192,2]{0,1:T(2,128)}, u32[]{:S(2)}) copy-start(f32[192,2]{0,1:T(2,128)} %param.15) | copy-start | bytes 4612
  1.8 99.1 %collective-permute-start = (bf16[256,2]{0,1:T(2,128)(2,1)S(1)}, bf16[256,2]{0,1:T(2,128)(2,1)S(1)}, u32[]{:S(2)}, u32[]{:S(2)}) collective-permute-start(bf16[256,2]{0,1:T(2,128)(2,1)S(1)} %slice.70), channel_id=1, source_target_pairs={{0,4},{4,8},{8,12},{12,16},{16,20},{20,24},{24,28},{1,5},{5,9},{9,... | collective-permute-start | bytes 3080 | tf_op jit(solution)/shard_map/ppermute | solution.py:310
  46.6 2.6 %copy-start.3 = (bf16[1,512,2048]{2,1,0:T(8,128)(2,1)S(1)}, bf16[1,512,2048]{2,1,0:T(8,128)(2,1)}, u32[]{:S(2)}) copy-start(bf16[1,512,2048]{2,1,0:T(8,128)(2,1)} %param.17) | copy-start | bytes 6291460
  46.6 2.6 %copy-start.5 = (bf16[1,8,48,2048]{3,2,1,0:T(8,128)(2,1)S(1)}, bf16[1,8,48,2048]{3,2,1,0:T(8,128)(2,1)}, u32[]{:S(2)}) copy-start(bf16[1,8,48,2048]{3,2,1,0:T(8,128)(2,1)} %get-tuple-element.19) | copy-start | bytes 4718596
  49.2 1.4 %copy-start.4 = (bf16[1,8,48,2048]{3,2,1,0:T(8,128)(2,1)S(1)}, bf16[1,8,48,2048]{3,2,1,0:T(8,128)(2,1)}, u32[]{:S(2)}) copy-start(bf16[1,8,48,2048]{3,2,1,0:T(8,128)(2,1)} %multiply_convert_fusion) | copy-start | bytes 4718596
  49.3 2.1 %copy-start.13 = (bf16[1,512,2048]{2,1,0:T(8,128)(2,1)S(1)}, bf16[1,512,2048]{2,1,0:T(8,128)(2,1)}, u32[]{:S(2)}) copy-start(bf16[1,512,2048]{2,1,0:T(8,128)(2,1)} %param.18) | copy-start | bytes 6291460
  56.3 2.6 %copy-start.1 = (f32[1,8,48,2048]{3,2,1,0:T(8,128)S(1)}, f32[1,8,48,2048]{3,2,1,0:T(8,128)}, u32[]{:S(2)}) copy-start(f32[1,8,48,2048]{3,2,1,0:T(8,128)} %get-tuple-element.18) | copy-start | bytes 9437188
  64.0 36.2 %copy-start.11 = (f32[3,256]{1,0:T(4,128)S(1)}, f32[3,256]{1,0:T(4,128)}, u32[]{:S(2)}) copy-start(f32[3,256]{1,0:T(4,128)} %param.22) | copy-start | bytes 9220
  64.0 37.0 %copy-start.7 = (bf16[256,192]{0,1:T(8,128)(2,1)S(1)}, bf16[256,192]{0,1:T(8,128)(2,1)}, u32[]{:S(2)}) copy-start(bf16[256,192]{0,1:T(8,128)(2,1)} %param.19) | copy-start | bytes 294916
  100.2 4.7 %copy-start.2 = (bf16[192,2048]{1,0:T(8,128)(2,1)S(1)}, bf16[192,2048]{1,0:T(8,128)(2,1)}, u32[]{:S(2)}) copy-start(bf16[192,2048]{1,0:T(8,128)(2,1)} %param.13) | copy-start | bytes 2359300
  103.6 19.5 %collective-permute-start.1 = (f32[256,2]{0,1:T(2,128)S(1)}, f32[256,2]{0,1:T(2,128)S(1)}, u32[]{:S(2)}, u32[]{:S(2)}) collective-permute-start(f32[256,2]{0,1:T(2,128)S(1)} %slice.74), channel_id=1, source_target_pairs={{4,0},{8,4},{12,8},{16,12},{20,16},{24,20},{28,24},{5,1},{9,5},{13... | collective-permute-start | bytes 6152 | tf_op jit(solution)/shard_map/ppermute | solution.py:310
  104.9 18.2 %copy-start.8 = (bf16[256,192]{0,1:T(8,128)(2,1)S(1)}, bf16[256,192]{0,1:T(8,128)(2,1)}, u32[]{:S(2)}) copy-start(bf16[256,192]{0,1:T(8,128)(2,1)} %param.20) | copy-start | bytes 294916
  104.9 19.0 %copy-start.9 = (bf16[256,192]{0,1:T(8,128)(2,1)S(1)}, bf16[256,192]{0,1:T(8,128)(2,1)}, u32[]{:S(2)}) copy-start(bf16[256,192]{0,1:T(8,128)(2,1)} %param.21) | copy-start | bytes 294916

commit v2 on v1

--- a/solution.py
+++ b/solution.py
@@ -41,39 +41,89 @@
     )
 
 
+def half(quarter, side, width):
+    return pl.ds(pl.multiple_of(quarter * width + side * (width // 2), width // 2), width // 2)
+
+
 def dispatch_kernel(
-    rows_ref, weight_ref, out_ref, weight_out, s1, r1, s2, r2, s3, r3, sw, rw, sp_, rp_, own
+    position_ref,
+    by_core_ref,
+    moe_ref,
+    cot_ref,
+    out_x,
+    out_cot,
+    rows,
+    weights,
+    landed,
+    weight_in,
+    s1,
+    r1,
+    s2,
+    r2,
+    s3,
+    r3,
+    s4,
+    r4,
+    sw,
+    rw,
+    sm,
+    rm,
+    own,
 ):
     s, t, z, c, lanes = place()
-    width = rows_ref.shape[-1] // 4
+    tokens, model = moe_ref.shape
+    cap = tokens // GROUPS
+    width = model // 4
     mate = (CORES * z + 1 - c, t)
     ahead = [lax.rem(z + d, GROUPS) for d in range(GROUPS)]
     behind = [lax.rem(z + GROUPS - d, GROUPS) for d in range(GROUPS)]
-    greet(
+    targets = (
         [(CORES * ahead[d] + c, t) for d in range(1, GROUPS)]
         + [(CORES * ahead[d] + 1 - c, t) for d in range(1, GROUPS)]
         + [(s, lanes[0]), (s, lanes[1]), mate]
     )
-    quarters = (t, lanes[2])
+    barrier = pltpu.get_barrier_semaphore()
+    for target in targets:
+        pl.semaphore_signal(barrier, inc=1, device_id=target, device_id_type=MESH)
+    select = position_ref[...] == lax.broadcasted_iota(jnp.int32, (tokens, tokens), 0)
+    permute = select.astype(jnp.float32).astype(jnp.bfloat16)
+    rows[:, 0] = (
+        jnp.dot(permute, moe_ref[...], preferred_element_type=jnp.float32)
+        .astype(rows.dtype)
+        .reshape(GROUPS, cap, model)
+    )
+    rows[:, 1] = (
+        jnp.dot(permute, cot_ref[...], preferred_element_type=jnp.float32)
+        .astype(rows.dtype)
+        .reshape(GROUPS, cap, model)
+    )
+    columns = [
+        jnp.sum(jnp.where(select, by_core_ref[k : k + 1, :], 0.0), axis=1, keepdims=True)
+        for k in range(CORES)
+    ]
+    lane_at = lax.broadcasted_iota(jnp.int32, (tokens, 128), 1)
+    weights[...] = jnp.where(lane_at == 0, columns[0], columns[1]).reshape(GROUPS, cap, 128)
+    pl.semaphore_wait(barrier, len(targets))
+
+    order = (2, 1, 3)
+    mine = span(t, width)
     first = {}
+    for d in order:
+        first[d] = remote(
+            rows.at[ahead[d], :, :, mine],
+            landed.at[:, s, :, mine],
+            s1.at[d - 1],
+            r1.at[d - 1],
+            (CORES * ahead[d] + c, t),
+        )
+        first[d].start()
     small = []
-    for d in (2, 1, 3):
-        for j in range(2):
-            cols = span(quarters[j], width)
-            copy = remote(
-                rows_ref.at[ahead[d], :, :, cols],
-                out_ref.at[:, s, :, cols],
-                s1.at[j, d - 1],
-                r1.at[j, d - 1],
-                (CORES * ahead[d] + c, t),
-            )
-            copy.start()
-            first[j, d] = copy
+    for d in order:
         for k in range(2):
             core = c if k == 0 else 1 - c
             copy = remote(
-                weight_ref.at[ahead[d]],
-                weight_out.at[s],
+                weights.at[ahead[d]],
+                weight_in.at[s],
                 sw.at[k, d - 1],
                 rw.at[k, d - 1],
                 (CORES * ahead[d] + core, t),
@@ -81,73 +131,94 @@
             copy.start()
             small.append(copy)
     pair = [
-        remote(rows_ref.at[z], out_ref.at[:, s], sp_.at[0], rp_.at[0], mate),
-        remote(weight_ref.at[z], weight_out.at[s], sp_.at[1], rp_.at[1], mate),
+        remote(rows.at[z], landed.at[:, s], sm.at[0], rm.at[0], mate),
+        remote(weights.at[z], weight_in.at[s], sm.at[1], rm.at[1], mate),
     ]
     local = [
-        pltpu.make_async_copy(rows_ref.at[z], out_ref.at[:, s], own.at[0]),
-        pltpu.make_async_copy(weight_ref.at[z], weight_out.at[s], own.at[1]),
+        pltpu.make_async_copy(rows.at[z], landed.at[:, s], own.at[0]),
+        pltpu.make_async_copy(weights.at[z], weight_in.at[s], own.at[1]),
     ]
     for copy in pair + local:
         copy.start()
-    order = (1, 3, 2)
+
+    def finish(source):
+        at_core = lax.broadcasted_iota(jnp.int32, (cap, 128), 1) == c
+        scale = jnp.sum(jnp.where(at_core, weight_in[source], 0.0), axis=1, keepdims=True)
+        out_x[source] = landed[0, source]
+        out_cot[source] = (scale * landed[1, source].astype(jnp.float32)).astype(out_cot.dtype)
+
     second = {}
     for d in order:
-        first[0, d].wait_recv()
-        cols = span(t, width)
-        block = out_ref.at[:, CORES * behind[d] + c, :, cols]
+        first[d].wait_recv()
+        block = landed.at[:, CORES * behind[d] + c, :, mine]
         for j in range(2):
-            copy = remote(block, block, s2.at[j, d - 1], r2.at[j, d - 1], (s, lanes[j]))
-            copy.start()
-            second[j, d] = copy
-    third = []
-    for d in order:
-        first[1, d].wait_recv()
-        second[0, d].wait_recv()
-        second[1, d].wait_recv()
-        block = out_ref.at[:, CORES * behind[d] + c]
-        copy = remote(block, block, s3.at[d - 1], r3.at[d - 1], mate)
-        copy.start()
-        third.append(copy)
+            second[j, d] = remote(
+                block, block, s2.at[j, d - 1], r2.at[j, d - 1], (s, lanes[j])
+            )
+            second[j, d].start()
+    third = {}
+    for d in order:
+        for j in range(2):
+            second[j, d].wait_recv()
+        for j in range(2):
+            block = landed.at[:, CORES * behind[d] + c, :, half(lanes[1 - j], j, width)]
+            third[j, d] = remote(
+                block, block, s3.at[j, d - 1], r3.at[j, d - 1], (s, lanes[j])
+            )
+            third[j, d].start()
     for copy in local:
         copy.wait()
-    for copy in small + pair + third:
+    finish(s)
+    for copy in pair:
         copy.wait()
-    for copy in list(first.values()) + list(second.values()):
-        copy.wait_send()
-
-
-def dispatch(rows, weights):
-    groups, two, cap, model = rows.shape
+    finish(CORES * z + 1 - c)
+    for copy in small:
+        copy.wait()
+    fourth = {}
+    for d in order:
+        for j in range(2):
+            third[j, d].wait_recv()
+        block = landed.at[:, CORES * behind[d] + c]
+        fourth[d] = remote(block, block, s4.at[d - 1], r4.at[d - 1], mate)
+        fourth[d].start()
+        finish(CORES * behind[d] + c)
+    for d in order:
+        fourth[d].wait_recv()
+        finish(CORES * behind[d] + 1 - c)
+    for group in (first, second, third, fourth):
+        for copy in group.values():
+            copy.wait_send()
+
+
+def dispatch(position, by_core, moe_in, cotangent):
+    tokens, model = moe_in.shape
+    cap = tokens // GROUPS
     vmem = pl.BlockSpec(memory_space=pltpu.VMEM)
     dma = pltpu.SemaphoreType.DMA
+    landing = jax.ShapeDtypeStruct((CORES * GROUPS, cap, model), moe_in.dtype)
+    one, two = (GROUPS - 1,), (2, GROUPS - 1)
     return pl.pallas_call(
         dispatch_kernel,
-        out_shape=(
-            jax.ShapeDtypeStruct((two, CORES * groups, cap, model), rows.dtype),
-            jax.ShapeDtypeStruct((CORES * groups,) + weights.shape[1:], weights.dtype),
-        ),
-        in_specs=[vmem, vmem],
+        out_shape=(landing, landing),
+        in_specs=[vmem] * 4,
         out_specs=(vmem, vmem),
         scratch_shapes=[
-            dma((2, groups - 1)),
-            dma((2, groups - 1)),
-            dma((2, groups - 1)),
-            dma((2, groups - 1)),
-            dma((groups - 1,)),
-            dma((groups - 1,)),
-            dma((2, groups - 1)),
-            dma((2, groups - 1)),
-            dma((2,)),
-            dma((2,)),
-            dma((2,)),
-        ],
+            pltpu.VMEM((GROUPS, 2, cap, model), moe_in.dtype),
+            pltpu.VMEM((GROUPS, cap, 128), jnp.float32),
+            pltpu.VMEM((2, CORES * GROUPS, cap, model), moe_in.dtype),
+            pltpu.VMEM((CORES * GROUPS, cap, 128), jnp.float32),
+        ]
+        + [dma(one), dma(one)]
+        + [dma(two) for _ in range(4)]
+        + [dma(one), dma(one)]
+        + [dma(two), dma(two)]
+        + [dma((2,)) for _ in range(3)],
         compiler_params=pltpu.CompilerParams(collective_id=0, has_side_effects=True),
         name="dispatch",
-    )(rows, weights)
-
-
-def combine_kernel(part_ref, out_ref, mate_in, total, lane_in, done, sa, ra, sb, rb, sc, rc, sd, rd):
+    )(position, by_core, moe_in, cotangent)
+
+
+def combine_kernel(part_ref, out_ref, mate_in, total, lane_in, done, sa, ra, sb, rb, sc, rc, sd, rd, se, re):
     s, t, z, c, lanes = place()
     width = part_ref.shape[-1] // 4
     mate = (CORES * z + 1 - c, t)
@@ -198,17 +269,27 @@
                 (CORES * ahead[d] + c, t),
             )
             home[d].start()
-    spread = []
+    spread = {}
     for d in (0, 1, 3, 2):
         if d:
             home[d].wait_recv()
         block = out_ref.at[behind[d], :, mine]
-        for j in (2, 0, 1):
-            copy = remote(block, block, sd.at[j, d], rd.at[j, d], (s, lanes[j]))
+        for j in range(2):
+            spread[j, d] = remote(block, block, sd.at[j, d], rd.at[j, d], (s, lanes[j]))
+            spread[j, d].start()
+    relay = []
+    for d in (0, 1, 3, 2):
+        for j in range(2):
+            spread[j, d].wait_recv()
+        for j in range(2):
+            block = out_ref.at[behind[d], :, half(lanes[1 - j], j, width)]
+            copy = remote(block, block, se.at[j, d], re.at[j, d], (s, lanes[j]))
             copy.start()
-            spread.append(copy)
-    for copy in spread:
+            relay.append(copy)
+    for copy in relay:
         copy.wait()
+    for copy in spread.values():
+        copy.wait_send()
     for copy in list(swap.values()) + list(across.values()) + list(home.values()):
         copy.wait_send()
 
@@ -234,15 +315,17 @@
             dma((3, groups)),
             dma((groups - 1,)),
             dma((groups - 1,)),
-            dma((3, groups)),
-            dma((3, groups)),
+            dma((2, groups)),
+            dma((2, groups)),
+            dma((2, groups)),
+            dma((2, groups)),
         ],
         compiler_params=pltpu.CompilerParams(collective_id=1, has_side_effects=True),
         name="combine",
     )(part)
 
 
-def project_kernel(part_ref, out_ref, mate_in, total, far_in, sa, ra, sb, rb):
+def project_kernel(part_ref, out_ref, far_in, mate_in, total, sa, ra, sb, rb):
     s, t, z, c, lanes = place()
     width = out_ref.shape[1]
     mate = (CORES * z + 1 - c, t)
@@ -273,9 +356,6 @@
             far[d].start()
     for d in range(1, GROUPS):
         far[d].wait_recv()
-    out_ref[...] += (
-        far_in[0].astype(jnp.float32) + far_in[1].astype(jnp.float32)
-    ) + far_in[2].astype(jnp.float32)
     for copy in list(swap.values()) + list(far.values()):
         copy.wait_send()
 
@@ -287,12 +367,14 @@
     dma = pltpu.SemaphoreType.DMA
     return pl.pallas_call(
         project_kernel,
-        out_shape=jax.ShapeDtypeStruct((channels, width), jnp.float32),
+        out_shape=(
+            jax.ShapeDtypeStruct((channels, width), jnp.float32),
+            jax.ShapeDtypeStruct((GROUPS - 1, channels, width), part.dtype),
+        ),
         in_specs=[vmem],
-        out_specs=vmem,
+        out_specs=(vmem, vmem),
         scratch_shapes=[
             pltpu.VMEM((GROUPS, channels, width), part.dtype),
-            pltpu.VMEM((GROUPS - 1, channels, width), part.dtype),
             pltpu.VMEM((GROUPS - 1, channels, width), part.dtype),
             dma((GROUPS,)),
             dma((GROUPS,)),
@@ -458,7 +540,6 @@
     lane_count = lax.axis_size("tp")
     model_width = moe_in.shape[1]
     cap = tok_rows // GROUPS
-    core = lax.rem(lax.axis_index("sp"), CORES)
     group = routing[:, 0] // CORES
     at = jnp.arange(tok_rows, dtype=jnp.int32)
     same = (group[:, None] == group[None, :]) & (at[:, None] < at[None, :])
@@ -472,24 +553,9 @@
             jnp.where(is_even, route_weight[:, 1], route_weight[:, 0]),
         ]
     )
-    weights = jnp.sum(jnp.where(select[None], by_core[:, None, :], 0.0), axis=2)
-    weights = weights.reshape(CORES, GROUPS, cap).transpose(1, 0, 2)
-    weights = jnp.pad(weights, ((0, 0), (0, 8 - CORES), (0, 128 - cap)))
-    rows = jnp.stack(
-        [
-            jnp.dot(permute, array, preferred_element_type=jnp.float32)
-            .astype(jnp.bfloat16)
-            .reshape(GROUPS, cap, model_width)
-            for array in (moe_in, cotangent)
-        ],
-        axis=1,
-    )
-    landed, landed_weights = dispatch(rows, weights)
-    arrived = landed[0].reshape(-1, model_width)
-    scales = lax.dynamic_index_in_dim(landed_weights, core, 1, False)[:, :cap].reshape(-1, 1)
-    arrived_cot = (scales * landed[1].reshape(-1, model_width).astype(jnp.float32)).astype(
-        jnp.bfloat16
-    )
+    landed, landed_cot = dispatch(position[None, :], by_core, moe_in, cotangent)
+    arrived = landed.reshape(-1, model_width)
+    arrived_cot = landed_cot.reshape(-1, model_width)
     contract_model = (((1,), (1,)), ((), ()))
     over_rows = (((0,), (0,)), ((), ()))
     gate_pre = lax.dot_general(
@@ -545,9 +611,10 @@
     act_grad = lax.dot_general(
         out_proj, stream_grad, contract_model, preferred_element_type=jnp.float32
     )
-    proj_grad = project(
+    near, far = project(
         jnp.dot(mixer_act, stream_grad, preferred_element_type=jnp.float32).astype(jnp.bfloat16)
     )
+    proj_grad = near + jnp.sum(far.astype(jnp.float32), axis=0)
     gate_b_grad = (act_grad * conv_out).astype(jnp.bfloat16)
     conv_grad = act_grad * gate_b.astype(jnp.float32)
     later = from_behind(conv_grad[:, : TAPS - 1], "sp", -1)

time: 127 us -> 112 us (0.88)
  Pallas kernels: 78.4 us -> 73.9 us
  other arithmetic: 13.8 us -> 9.51 us
  local copies, waits for them, and re-layouts: 5.03 us -> 1.76 us
  matrix products: 24.4 us -> 21.5 us
    pallas_call x1, Pallas kernels: 34.7 us -> 26.4 us  [combine(): pl.pallas_call(combine_kernel, out_shape=jax.ShapeDtypeStruct((groups, ca...]
    convert_element_type x3 -> x0, other arithmetic: 7.77 us -> none  [the longest x1 4.67 us: on_device_paired(): landed[1].reshape(-1, model_width).astype(jnp.float32)]
    pallas_call x2, Pallas kernels: 43.7 us -> 47.5 us  [the longest x1 30.7 us: dispatch(): pl.pallas_call(dispatch_kernel, out_shape=(landing, landing), in_specs=[v...]
    dot_general x2 -> x0, matrix products: 2.75 us -> none  [on_device_paired(): jnp.dot(permute, array, preferred_element_type=jnp.float32)]
    another operation x1 -> x0, other arithmetic: 2.43 us -> none  [on_device_paired(): jnp.stack([jnp.dot(permute, array, preferred_element_type=jnp.float32).as...]
    unnamed x29 -> x20, local copies, waits for them, and re-layouts: 2.78 us -> 1.05 us
    add x0 -> x1, other arithmetic: none -> 1.7 us  [on_device_paired(): proj_grad = near + jnp.sum(far.astype(jnp.float32), axis=0)]
  transfers between devices with their start and end apart: 2 -> 2, of which waited for: 0 -> 0; matrix products, arithmetic and copies ran while one was open for 28% -> 24% of each run, Pallas kernels for 62% -> 66%
where the time goes in v2:
time: 112 us; the launch traced here: 111 us
  Pallas kernels  73.9 us (66%)
  matrix products  21.5 us (19%)
  other arithmetic  9.51 us (8%)
  starting transfers between devices  3.68 us (3%)
  local copies, waits for them, and re-layouts  1.76 us (2%)
    pallas_call x1, Pallas kernels, dispatch(): pl.pallas_call(dispatch_kernel, out_shape=(landing, landing), in_specs=[v...  30.7 us
    pallas_call x1, Pallas kernels, combine(): pl.pallas_call(combine_kernel, out_shape=jax.ShapeDtypeStruct((groups, ca...  26.4 us
    pallas_call x1, Pallas kernels, project(): pl.pallas_call(project_kernel, out_shape=(jax.ShapeDtypeStruct((channels,...  16.8 us
    ppermute x2, starting transfers between devices, from_behind(): return lax.ppermute(array, axis, pairs)  3.68 us
    dot_general x1, matrix products, on_device_paired(): lax.dot_general(hidden, arrived_cot, over_rows, preferred_element_type=jn...  2.66 us
    dot_general x1, matrix products, on_device_paired(): lax.dot_general(out_proj, stream_grad, contract_model, preferred_element_...  2.66 us
    dot_general x1, matrix products, on_device_paired(): lax.dot_general(gate_grad, arrived, over_rows, preferred_element_type=jnp...  2.61 us
    dot_general x1, matrix products, on_device_paired(): lax.dot_general(up_grad, arrived, over_rows, preferred_element_type=jnp.f...  2.6 us
  transfers between devices with their start and end apart: 2, of which 0 were waited for; matrix products, arithmetic and copies ran while one was open for 24% of the time, Pallas kernels for 66%

profile of v2, /device:TPU:0, one launch (start us, length us, event | category | flops | bytes accessed | tf_op | source)
XLA Modules:
  0.0 111.2 jit_solution(13868044009711124664)
XLA Ops:
  0.6 0.0 copy-start
  0.6 1.1 %fusion.19 = bf16[256,192]{0,1:T(8,128)(2,1)S(1)} fusion(bf16[256,192]{0,1:T(8,128)(2,1)} %param.21, bf16[256,192]{0,1:T(8,128)(2,1)} %param.20), kind=kLoop, calls=%fused_computation.39 | loop fusion | flops 196608 | bytes 294912 | tf_op jit(solution)/shard_map/convert_element_type | solution.py:603
  1.8 2.4 %collective-permute-start = (bf16[256,2]{0,1:T(2,128)(2,1)S(1)}, bf16[256,2]{0,1:T(2,128)(2,1)S(1)}, u32[]{:S(2)}, u32[]{:S(2)}) collective-permute-start(bf16[256,2]{0,1:T(2,128)(2,1)S(1)} %slice.58), channel_id=1, source_target_pairs={{0,4},{4,8},{8,12},{12,16},{16,20},{20,24},{24,28},{1,5},{5,9},{9,... | collective-permute-start | bytes 3080 | tf_op jit(solution)/shard_map/ppermute | solution.py:392
  4.2 0.7 and_select_fusion.1
  4.9 0.8 compare_select_fusion.7
  5.7 0.8 compare_select_fusion.6
  6.4 0.1 convert_reduce_fusion.1
  6.6 1.3 %multiply_add_fusion.1.position_ref = s32[1,192]{1,0:T(1,128)} fusion(s32[1,192]{1,0:T(1,128)S(1)} %bitcast.75, s32[1,192]{1,0:T(1,128)S(1)} %get-tuple-element.21, s32[192,2]{0,1:T(2,128)} %param.14), kind=kLoop, calls=%fused_computation.73 | loop fusion | flops 2688 | bytes 3072 | tf_op jit(solution)/shard_map/add | solution.py:546
  7.8 0.6 pad_maximum_fusion.1.by_core_ref
  8.4 30.7 %dispatch.1 = (bf16[8,48,2048]{2,1,0:T(8,128)(2,1)}, bf16[8,48,2048]{2,1,0:T(8,128)(2,1)}) custom-call(s32[1,192]{1,0:T(1,128)} %multiply_add_fusion.1.position_ref, f32[2,192]{1,0:T(2,128)} %pad_maximum_fusion.1.by_core_ref, bf16[192,2048]{1,0:T(8,128)(2,1)} %moe_ref.1, bf16[192,2048]{1,0:T(8,128)(2,1)} %cot_ref.1), custom_call_target="tpu_custom_call" | custom-call | tf_op jit(solution)/shard_map/dispatch/pallas_call | solution.py:200
  39.1 0.0 copy-done
  39.1 0.0 copy-start.2
  39.1 0.0 copy-start.8
  39.1 2.6 %fusion.5 = f32[384,512]{1,0:T(8,128)S(1)} fusion(bf16[384,2048]{1,0:T(8,128)(2,1)} %bitcast.77, bf16[1,512,2048]{2,1,0:T(8,128)(2,1)S(1)} %copy-done), kind=kOutput, calls=%fused_computation.11 | convolution fusion | flops 805306368 | bytes 4456448 | tf_op jit(solution)/shard_map/dot_general | solution.py:561
  41.7 0.0 copy-done.2
  41.7 0.0 copy-done.8
  41.7 0.0 copy-start.7
  41.7 0.0 copy-start.9
  41.7 1.0 fusion.8
  42.7 0.6 copy-done.7
  43.3 0.4 copy-done.9
  43.7 1.2 %multiply_convert_fusion.1 = (bf16[384,512]{1,0:T(8,128)(2,1)S(1)}, bf16[384,512]{1,0:T(8,128)(2,1)S(1)}) fusion(f32[384,512]{1,0:T(8,128)S(1)} %fusion.5, f32[384,512]{1,0:T(8,128)S(1)} %fusion.8, bf16[384,2048]{1,0:T(8,128)(2,1)S(1)} %bitcast.81, bf16[1,512,2048]{2,1,0:T(8,128)(2,1)S(1)} %copy-done.7), kind=kOutput, calls=%fused_computation.22 | convolution fusion | flops 807862272 | bytes 6029312 | tf_op jit(solution)/shard_map/dot_general | solution.py:567
  45.0 1.0 fusion.3
  45.9 2.6 %fusion = bf16[1,512,2048]{2,1,0:T(8,128)(2,1)} fusion(bf16[384,512]{1,0:T(8,128)(2,1)S(1)} %get-tuple-element.23, bf16[384,2048]{1,0:T(8,128)(2,1)S(1)} %bitcast.79), kind=kOutput, calls=%fused_computation.4 | convolution fusion | flops 806354944 | bytes 4063232 | tf_op jit(solution)/shard_map/dot_general | solution.py:574
  48.5 2.7 %fusion.2 = bf16[1,512,2048]{2,1,0:T(8,128)(2,1)} fusion(bf16[384,2048]{1,0:T(8,128)(2,1)S(1)} %bitcast.82, f32[384,512]{1,0:T(8,128)S(1)} %fusion.8, f32[384,512]{1,0:T(8,128)S(1)} %fusion.5), kind=kOutput, calls=%fused_computation.6 | convolution fusion | flops 807534592 | bytes 5242880 | tf_op jit(solution)/shard_map/dot_general | solution.py:580
  51.2 2.6 %fusion.1 = bf16[1,512,2048]{2,1,0:T(8,128)(2,1)} fusion(bf16[384,512]{1,0:T(8,128)(2,1)S(1)} %get-tuple-element.22, bf16[384,2048]{1,0:T(8,128)(2,1)S(1)} %bitcast.80), kind=kOutput, calls=%fused_computation.5 | convolution fusion | flops 806354944 | bytes 4063232 | tf_op jit(solution)/shard_map/dot_general | solution.py:577
  53.8 2.2 %add_convert_fusion = bf16[384,2048]{1,0:T(8,128)(2,1)} fusion(f32[384,2048]{1,0:T(8,128)S(1)} %fusion.3, bf16[384,512]{1,0:T(8,128)(2,1)S(1)} %get-tuple-element.22, bf16[1,512,2048]{2,1,0:T(8,128)(2,1)S(1)} %copy-done.2), kind=kOutput, calls=%fused_computation | convolution fusion | flops 806879232 | bytes 7208960 | tf_op jit(solution)/shard_map/dot_general | solution.py:583
  56.0 0.0 copy-start.6
  56.0 0.0 copy-start.3
  56.0 26.4 %combine.1 = bf16[4,48,2048]{2,1,0:T(8,128)(2,1)} custom-call(bf16[4,2,48,2048]{3,2,1,0:T(8,128)(2,1)} %bitcast.65), custom_call_target="tpu_custom_call" | custom-call | tf_op jit(solution)/shard_map/combine/pallas_call | solution.py:302
  82.4 0.0 copy-done.6
  82.4 1.6 %convolution_convert_fusion.4 = bf16[192,2048]{1,0:T(8,128)(2,1)S(1)} fusion(bf16[192,2048]{1,0:T(8,128)(2,1)} %bitcast.66, s32[192]{0:T(256)S(1)} %multiply_add_fusion), kind=kOutput, calls=%fused_computation.8 | convolution fusion | flops 151425024 | bytes 1573632 | tf_op jit(solution)/shard_map/dot_general | solution.py:589
  84.0 0.0 copy-start.1
  84.0 0.7 constant_dynamic-slice_fusion
  84.7 0.0 collective-permute-done
  84.7 0.0 copy-done.3
  84.7 2.7 %multiply_convert_fusion.4 = (bf16[256,192]{0,1:T(8,128)(2,1)}, f32[256,192]{0,1:T(8,128)S(1)}, f32[256,192]{0,1:T(8,128)S(1)}) fusion(f32[256,194]{0,1:T(8,128)S(1)} %maximum_convert_fusion, f32[256]{0:T(256)S(1)} %bitcast.69, f32[256]{0:T(256)S(1)} %bitcast.71, f32[256]{0:T(256)S(1)} %bitcast.67, bf16[256,192]{0,1:T(8,128)(2,1)S(1)} %copy-done.3, ...), kind=kOutput, calls=%fused_computation.48 | convolution fusion | flops 203341824 | bytes 3804160 | tf_op jit(solution)/shard_map/dot_general | solution.py:611
  87.4 1.3 %collective-permute-start.1 = (f32[256,2]{0,1:T(2,128)S(1)}, f32[256,2]{0,1:T(2,128)S(1)}, u32[]{:S(2)}, u32[]{:S(2)}) collective-permute-start(f32[256,2]{0,1:T(2,128)S(1)} %slice.62), channel_id=1, source_target_pairs={{4,0},{8,4},{12,8},{16,12},{20,16},{24,20},{28,24},{5,1},{9,5},{13... | collective-permute-start | bytes 6152 | tf_op jit(solution)/shard_map/ppermute | solution.py:392
  88.7 0.0 copy-done.1
  88.7 0.0 copy-start.4
  88.7 1.5 %convolution_convert_fusion.3.part_ref = bf16[256,2048]{1,0:T(8,128)(2,1)} fusion(bf16[192,2048]{1,0:T(8,128)(2,1)S(1)} %convolution_convert_fusion.4, bf16[192,2048]{1,0:T(8,128)(2,1)S(1)} %copy-done.1, f32[256,192]{0,1:T(8,128)S(1)} %get-tuple-element.19, bf16[256,192]{0,1:T(8,128)(2,1)S(1)} %copy-done.3), kind=kOutput, calls=%fused_computation.7 | convolution fusion | flops 203571200 | bytes 2916352 | tf_op jit(solution)/shard_map/dot_general | solution.py:615
  90.2 0.0 copy-start.5
  90.2 16.8 %project.1 = (f32[256,256]{1,0:T(8,128)}, bf16[3,256,256]{2,1,0:T(8,128)(2,1)}) custom-call(bf16[256,2048]{1,0:T(8,128)(2,1)} %convolution_convert_fusion.3.part_ref), custom_call_target="tpu_custom_call" | custom-call | tf_op jit(solution)/shard_map/project/pallas_call | solution.py:368
  107.0 1.1 convert_reduce_fusion
  108.1 1.7 %add.83 = f32[256,256]{1,0:T(8,128)} add(f32[256,256]{1,0:T(8,128)} %get-tuple-element.14, f32[256,256]{1,0:T(8,128)S(1)} %convert_reduce_fusion) | non-fusion elementwise | flops 65536 | bytes 786432 | tf_op jit(solution)/shard_map/add | solution.py:617
  109.8 0.0 collective-permute-done.1
  109.8 0.0 copy-done.4
  109.8 0.7 fusion.18
  110.5 0.0 copy-done.5
  110.5 0.7 fusion.20
  (6 shorter events, 0.1 us)
Async XLA Ops:
  0.6 38.4 %copy-start = (bf16[1,512,2048]{2,1,0:T(8,128)(2,1)S(1)}, bf16[1,512,2048]{2,1,0:T(8,128)(2,1)}, u32[]{:S(2)}) copy-start(bf16[1,512,2048]{2,1,0:T(8,128)(2,1)} %param.16) | copy-start | bytes 6291460
  1.8 82.9 %collective-permute-start = (bf16[256,2]{0,1:T(2,128)(2,1)S(1)}, bf16[256,2]{0,1:T(2,128)(2,1)S(1)}, u32[]{:S(2)}, u32[]{:S(2)}) collective-permute-start(bf16[256,2]{0,1:T(2,128)(2,1)S(1)} %slice.58), channel_id=1, source_target_pairs={{0,4},{4,8},{8,12},{12,16},{16,20},{20,24},{24,28},{1,5},{5,9},{9,... | collective-permute-start | bytes 3080 | tf_op jit(solution)/shard_map/ppermute | solution.py:392
  39.1 2.6 %copy-start.2 = (bf16[1,512,2048]{2,1,0:T(8,128)(2,1)S(1)}, bf16[1,512,2048]{2,1,0:T(8,128)(2,1)}, u32[]{:S(2)}) copy-start(bf16[1,512,2048]{2,1,0:T(8,128)(2,1)} %param.17) | copy-start | bytes 6291460
  39.1 2.6 %copy-start.8 = (bf16[8,48,2048]{2,1,0:T(8,128)(2,1)S(1)}, bf16[8,48,2048]{2,1,0:T(8,128)(2,1)}, u32[]{:S(2)}) copy-start(bf16[8,48,2048]{2,1,0:T(8,128)(2,1)} %get-tuple-element.13) | copy-start | bytes 4718596
  41.7 1.6 %copy-start.7 = (bf16[1,512,2048]{2,1,0:T(8,128)(2,1)S(1)}, bf16[1,512,2048]{2,1,0:T(8,128)(2,1)}, u32[]{:S(2)}) copy-start(bf16[1,512,2048]{2,1,0:T(8,128)(2,1)} %param.18) | copy-start | bytes 6291460
  41.7 2.0 %copy-start.9 = (bf16[8,48,2048]{2,1,0:T(8,128)(2,1)S(1)}, bf16[8,48,2048]{2,1,0:T(8,128)(2,1)}, u32[]{:S(2)}) copy-start(bf16[8,48,2048]{2,1,0:T(8,128)(2,1)} %get-tuple-element.12) | copy-start | bytes 4718596
  56.0 26.4 %copy-start.6 = (f32[3,256]{1,0:T(4,128)S(1)}, f32[3,256]{1,0:T(4,128)}, u32[]{:S(2)}) copy-start(f32[3,256]{1,0:T(4,128)} %param.22) | copy-start | bytes 9220
  56.0 28.7 %copy-start.3 = (bf16[256,192]{0,1:T(8,128)(2,1)S(1)}, bf16[256,192]{0,1:T(8,128)(2,1)}, u32[]{:S(2)}) copy-start(bf16[256,192]{0,1:T(8,128)(2,1)} %param.19) | copy-start | bytes 294916
  84.0 4.7 %copy-start.1 = (bf16[192,2048]{1,0:T(8,128)(2,1)S(1)}, bf16[192,2048]{1,0:T(8,128)(2,1)}, u32[]{:S(2)}) copy-start(bf16[192,2048]{1,0:T(8,128)(2,1)} %cot_ref.1) | copy-start | bytes 2359300
  87.4 22.4 %collective-permute-start.1 = (f32[256,2]{0,1:T(2,128)S(1)}, f32[256,2]{0,1:T(2,128)S(1)}, u32[]{:S(2)}, u32[]{:S(2)}) collective-permute-start(f32[256,2]{0,1:T(2,128)S(1)} %slice.62), channel_id=1, source_target_pairs={{4,0},{8,4},{12,8},{16,12},{20,16},{24,20},{28,24},{5,1},{9,5},{13... | collective-permute-start | bytes 6152 | tf_op jit(solution)/shard_map/ppermute | solution.py:392
  88.7 21.1 %copy-start.4 = (bf16[256,192]{0,1:T(8,128)(2,1)S(1)}, bf16[256,192]{0,1:T(8,128)(2,1)}, u32[]{:S(2)}) copy-start(bf16[256,192]{0,1:T(8,128)(2,1)} %param.20) | copy-start | bytes 294916
  90.2 20.4 %copy-start.5 = (bf16[256,192]{0,1:T(8,128)(2,1)S(1)}, bf16[256,192]{0,1:T(8,128)(2,1)}, u32[]{:S(2)}) copy-start(bf16[256,192]{0,1:T(8,128)(2,1)} %param.21) | copy-start | bytes 294916
